TPU v7x, 128 devices: a whole 4x4x4 slice. The times are simulated.
128 devices in a mesh: sp: 64 (over z, y, x), tp: 2 (over core).
Axes of the slice: x: 4, y: 4, z: 4, core: 2. Of those that a mesh axis runs over, the one named last changes fastest.
Arguments:
- queries_narrow: bfloat16 [16384, 1024], P('sp', 'tp'), may hold values from -40 to 40
- keys_narrow: bfloat16 [16384, 256], P('sp', 'tp'), may hold values from -40 to 40
- values_narrow: bfloat16 [16384, 256], P('sp', 'tp'), may hold values from -6 to 6
- queries_wide: bfloat16 [16384, 1024], P('sp', 'tp'), may hold values from -40 to 40
- keys_wide: bfloat16 [16384, 512], P('sp', 'tp'), may hold values from -40 to 40
- values_wide: bfloat16 [16384, 512], P('sp', 'tp'), may hold values from -6 to 6
- lambda_narrow: float32 [8], P('tp'), may hold values from 0.3 to 0.8
- lambda_wide: float32 [4], P('tp'), may hold values from 0.3 to 0.8
- gain_narrow: float32 [128], replicated, may hold values from 0.1 to 1.9
- gain_wide: float32 [256], replicated, may hold values from 0.1 to 1.9
- out_narrow: bfloat16 [1024, 2048], replicated, may hold values from -0.125 to 0.125
- out_wide: bfloat16 [1024, 2048], replicated, may hold values from -0.125 to 0.125
- stream: bfloat16 [16384, 2048], P(('sp', 'tp')), may hold values from -6 to 6
- gain_mix: float32 [2048], replicated, may hold values from 0.1 to 1.9
- gain_ffn: float32 [2048], replicated, may hold values from 0.1 to 1.9
- gain_post: float32 [2048], replicated, may hold values from 0.1 to 1.9
- shared_gate: bfloat16 [2048, 512], replicated, may hold values from -0.125 to 0.125
- shared_up: bfloat16 [2048, 512], replicated, may hold values from -0.125 to 0.125
- shared_down: bfloat16 [512, 2048], replicated, may hold values from -0.25 to 0.25
- expert_gate: bfloat16 [128, 2048, 512], P('sp', None, 'tp'), may hold values from -0.125 to 0.125
- expert_up: bfloat16 [128, 2048, 512], P('sp', None, 'tp'), may hold values from -0.125 to 0.125
- expert_down: bfloat16 [128, 512, 2048], P('sp', 'tp'), may hold values from -0.25 to 0.25
- expert_ids: int32 [16384, 4], P(('sp', 'tp')), may hold values from 0 to 127, all different within a row; in each aligned block of 128 rows (0 to 127, 128 to 255, ...) at most 6 rows name the same one
- route_weights: float32 [16384, 4], P(('sp', 'tp')), may hold values from 0.2 to 1
Outputs:
- layer_out: bfloat16 [16384, 2048], P(('sp', 'tp'))
Inputs may be any that keep to these rules, and one draw needn't show every extreme that they name: `expert_ids`: the experts of one token differ. Within the rows that one device holds (aligned blocks of rows in the placement's order), no expert is named more than 6 times, and in every draw some expert is named exactly 6 times there.
All inputs are finite; a program needn't handle non-finite values.
Results may differ from a plain program's by a relative error of at most 0.015.
Values may be sent and summed in bfloat16 or wider, within the bound.
A program may use at most 192 MiB of HBM per device.

v0:
```python
import math

import jax
import jax.numpy as jnp
from jax import lax
from jax.sharding import PartitionSpec as P

D = 2048
DN = 64
VN = 128
DW = 128
VW = 256
TOPK = 4


EPS = 1e-06


def in_one_piece(arrays, axis, dim, along):
    ends, at = ([], 0)
    for a in arrays[:-1]:
        at += a.shape[along]
        ends.append(at)
    both = jnp.concatenate(arrays, axis=along)
    return tuple(jnp.split(lax.all_gather(both, axis, axis=dim, tiled=True), ends, axis=along))


def in_order(pieces, dim):
    pieces = jnp.moveaxis(pieces, 0, dim)
    dims = pieces.shape
    return pieces.reshape(*dims[:dim], dims[dim] * dims[dim + 1], *dims[dim + 2 :])


def sent_to_all(value, axis):
    peers = lax.axis_size(axis)
    return lax.all_to_all(
        jnp.broadcast_to(value[None], (peers, *value.shape)), axis, 0, 0, tiled=True
    )


def gathered_copies(value, axis, dim):
    return in_order(sent_to_all(value, axis), dim)


def in_blocks(value, dim, peers):
    before, after = (value.shape[:dim], value.shape[dim + 1 :])
    return jnp.moveaxis(value.reshape(*before, peers, -1, *after), dim, 0)


def sum_at_owner(value, axis, dim):
    pieces = in_blocks(value, dim, lax.axis_size(axis))
    arrived = lax.all_to_all(pieces, axis, split_axis=0, concat_axis=0, tiled=True)
    return arrived.astype(jnp.float32).sum(axis=0)


def rms_scale(values, gain_row):
    return values * lax.rsqrt(jnp.mean(values * values, axis=-1, keepdims=True) + EPS) * gain_row


def empty_state(groups, per_group, query_count, value_dim):
    return (
        jnp.full((groups, per_group, 2, query_count), -1e30, jnp.float32),
        jnp.zeros((groups, per_group, 2, query_count), jnp.float32),
        jnp.zeros((groups, per_group, 2, query_count, value_dim), jnp.float32),
    )


def attend_block(carried, query_heads, key_rows, value_rows, query_pos, key_pos, key_dim):
    row_max, row_sum, accumulated = carried
    scores = jnp.einsum(
        "qcgmd,kcmd->cgmqk", query_heads, key_rows, preferred_element_type=jnp.float32
    ) * key_dim ** (-0.5)
    causal = key_pos[None, :] <= query_pos[:, None]
    scores = jnp.where(causal, scores, -1e30)
    newmax = jnp.maximum(row_max, jnp.max(scores, axis=-1))
    weights = jnp.where(causal, jnp.exp(scores - newmax[..., None]), 0.0)
    factor = jnp.exp(row_max - newmax)
    row_sum = row_sum * factor + jnp.sum(weights, axis=-1)
    accumulated = accumulated * factor[..., None] + jnp.einsum(
        "cgmqk,kcv->cgmqv",
        weights.astype(jnp.bfloat16),
        value_rows,
        preferred_element_type=jnp.float32,
    )
    return (newmax, row_sum, accumulated)


def finish_group(carried, lam_heads, gain_row, value_dim):
    row_max, row_sum, accumulated = carried
    mapped = accumulated / row_sum[..., None]
    groups = mapped.shape[0]
    per_group = mapped.shape[1]
    lam_grid = lam_heads.reshape(groups, per_group)[:, :, None, None]
    difference = mapped[:, :, 0] - lam_grid * mapped[:, :, 1]
    normed = rms_scale(difference, gain_row)
    query_count = normed.shape[2]
    return (
        normed.transpose(2, 0, 1, 3)
        .reshape(query_count, groups * per_group * value_dim)
        .astype(jnp.bfloat16)
    )


def run_experts(incoming, expert_gate, expert_up, expert_down, capacity):
    sources = incoming.shape[0]
    local_experts = expert_gate.shape[0]
    grouped = incoming.reshape(sources, local_experts, capacity, D)
    gate_part = jnp.einsum(
        "rjcd,jdf->rjcf", grouped, expert_gate, preferred_element_type=jnp.float32
    )
    up_part = jnp.einsum("rjcd,jdf->rjcf", grouped, expert_up, preferred_element_type=jnp.float32)
    hidden = (jax.nn.silu(gate_part) * up_part).astype(jnp.bfloat16)
    result = jnp.einsum("rjcf,jfd->rjcd", hidden, expert_down, preferred_element_type=jnp.float32)
    return result.reshape(sources, local_experts * capacity, D)


def shards(
    queries_narrow,
    keys_narrow,
    values_narrow,
    queries_wide,
    keys_wide,
    values_wide,
    lambda_narrow,
    lambda_wide,
    gain_narrow,
    gain_wide,
    out_narrow,
    out_wide,
    stream,
    gain_mix,
    gain_ffn,
    gain_post,
    shared_gate,
    shared_up,
    shared_down,
    expert_gate,
    expert_up,
    expert_down,
    expert_ids,
    route_weights,
):
    query_count = queries_narrow.shape[0]
    sp_index = lax.axis_index("sp")
    sp_count = lax.axis_size("sp")
    offset = sp_index * query_count
    narrow_groups = keys_narrow.shape[1] // (2 * DN)
    wide_groups = keys_wide.shape[1] // (2 * DW)
    query_sets = (queries_narrow, queries_wide, offset + jnp.arange(query_count, dtype=jnp.int32))
    prepared = []
    narrow_part, wide_part, positions = query_sets
    rows = narrow_part.shape[0]
    prepared.append(
        (
            narrow_part.reshape(rows, narrow_groups, -1, 2, DN),
            wide_part.reshape(rows, wide_groups, -1, 2, DW),
            positions,
            positions[rows - 1],
        )
    )
    initial = tuple(
        (
            (
                empty_state(narrow_groups, item[0].shape[2], item[0].shape[0], VN),
                empty_state(wide_groups, item[1].shape[2], item[1].shape[0], VW),
            )
            for item in prepared
        )
    )
    pieces = in_one_piece((keys_narrow, values_narrow, keys_wide, values_wide), "sp", 0, 1)
    key_count = pieces[0].shape[0]
    block_rows = math.gcd(key_count, 1024)
    narrow_keys = pieces[0].reshape(key_count, narrow_groups, 2, DN)
    narrow_values = pieces[1].reshape(key_count, narrow_groups, VN)
    wide_keys = pieces[2].reshape(key_count, wide_groups, 2, DW)
    wide_values = pieces[3].reshape(key_count, wide_groups, VW)

    def step_block(block_index, running):
        block_begin = block_index * block_rows
        key_pos = block_begin + jnp.arange(block_rows, dtype=jnp.int32)

        def take_rows(data):
            return lax.dynamic_slice_in_dim(data, block_begin, block_rows, 0)

        narrow_heads, wide_heads, positions, last_query = prepared[0]

        def update(
            carried_in, narrow_heads=narrow_heads, wide_heads=wide_heads, positions=positions
        ):
            return (
                attend_block(
                    carried_in[0],
                    narrow_heads,
                    take_rows(narrow_keys),
                    take_rows(narrow_values),
                    positions,
                    key_pos,
                    DN,
                ),
                attend_block(
                    carried_in[1],
                    wide_heads,
                    take_rows(wide_keys),
                    take_rows(wide_values),
                    positions,
                    key_pos,
                    DW,
                ),
            )

        def unchanged(carried_in):
            return carried_in

        updated = [lax.cond(block_begin <= last_query, update, unchanged, running[0])]
        return tuple(updated)

    states = lax.fori_loop(0, key_count // block_rows, step_block, initial)
    finished = [
        (
            finish_group(state[0], lambda_narrow, gain_narrow, VN),
            finish_group(state[1], lambda_wide, gain_wide, VW),
        )
        for state in states
    ]
    narrow_out, wide_out = finished[0]
    narrow_rows, wide_rows = (
        lax.all_to_all(narrow_out, "tp", split_axis=0, concat_axis=1, tiled=True),
        lax.all_to_all(wide_out, "tp", split_axis=0, concat_axis=1, tiled=True),
    )
    projected = jnp.dot(narrow_rows, out_narrow, preferred_element_type=jnp.float32) + jnp.dot(
        wide_rows, out_wide, preferred_element_type=jnp.float32
    )
    mixed_rows = (stream.astype(jnp.float32) + rms_scale(projected, gain_mix)).astype(jnp.bfloat16)
    normed = rms_scale(mixed_rows.astype(jnp.float32), gain_ffn).astype(jnp.bfloat16)
    row_count = normed.shape[0]
    tp_count = lax.axis_size("tp")
    local_experts = expert_gate.shape[0]
    experts_all = local_experts * sp_count
    capacity = max(2, 3 * row_count * TOPK // (2 * experts_all))
    flat_ids = expert_ids.reshape(-1)
    onehot = (flat_ids[:, None] == jnp.arange(experts_all, dtype=jnp.int32)[None, :]).astype(
        jnp.int32
    )
    earlier = jnp.cumsum(onehot, axis=0) - onehot
    slot_rank = jnp.sum(earlier * onehot, axis=1)
    slot_index = flat_ids * capacity + slot_rank
    buffer_rows = experts_all * capacity
    selector = slot_index[None, :] == jnp.arange(buffer_rows, dtype=jnp.int32)[:, None]
    selector = jnp.any(selector.reshape(buffer_rows, row_count, TOPK), axis=2).astype(jnp.bfloat16)
    outgoing = jnp.dot(selector, normed, preferred_element_type=jnp.float32).astype(jnp.bfloat16)
    outgoing = outgoing.reshape(sp_count, local_experts * capacity, D)
    incoming = lax.all_to_all(outgoing, "sp", split_axis=0, concat_axis=0, tiled=True)
    all_rows = gathered_copies(incoming[None], "tp", 0)
    partials = run_experts(
        all_rows.reshape(tp_count * sp_count, local_experts * capacity, D),
        expert_gate,
        expert_up,
        expert_down,
        capacity,
    )
    partials = partials.reshape(tp_count, sp_count, local_experts * capacity, D)
    own_sums = sum_at_owner(partials.astype(jnp.bfloat16), "tp", 0)
    returned = lax.all_to_all(
        own_sums[0].astype(jnp.bfloat16), "sp", split_axis=0, concat_axis=0, tiled=True
    )
    returned = returned.reshape(buffer_rows, D)
    picked = jnp.take(returned, slot_index, axis=0).reshape(row_count, TOPK, D)
    routed = jnp.einsum(
        "rk,rkd->rd", route_weights, picked.astype(jnp.float32), precision=lax.Precision.HIGHEST
    )
    shared_hidden = (
        jax.nn.silu(jnp.dot(normed, shared_gate, preferred_element_type=jnp.float32))
        * jnp.dot(normed, shared_up, preferred_element_type=jnp.float32)
    ).astype(jnp.bfloat16)
    shared_out = jnp.dot(shared_hidden, shared_down, preferred_element_type=jnp.float32)
    combined = shared_out + routed
    return (mixed_rows.astype(jnp.float32) + rms_scale(combined, gain_post)).astype(jnp.bfloat16)


def solution(mesh):
    return jax.shard_map(
        shards,
        mesh=mesh,
        in_specs=(
            P("sp", "tp"),
            P("sp", "tp"),
            P("sp", "tp"),
            P("sp", "tp"),
            P("sp", "tp"),
            P("sp", "tp"),
            P("tp"),
            P("tp"),
            P(),
            P(),
            P(),
            P(),
            P(("sp", "tp"), None),
            P(),
            P(),
            P(),
            P(),
            P(),
            P(),
            P("sp", None, "tp"),
            P("sp", None, "tp"),
            P("sp", "tp", None),
            P(("sp", "tp"), None),
            P(("sp", "tp"), None),
        ),
        out_specs=P(("sp", "tp"), None),
        check_vma=False,
    )
```

profile of v0, /device:TPU:1, one launch (start us, length us, event | category | flops | bytes accessed | tf_op | source)
XLA Modules:
  0.0 741.5 jit_solution(13892753805381695486)
XLA Ops:
  16.6 179.5 %all-gather.2.cloned.1.call-done = bf16[16384,768]{0,1:T(8,128)(2,1)} async-done(((bf16[256,768]{0,1:T(8,128)(2,1)}), bf16[16384,768]{0,1:T(8,128)(2,1)}) %all-gather.2.cloned.1.call-update) | async-done | bytes 25165840 | tf_op jit(solution)/shard_map/all_gather | solution.py:25
  196.1 11.5 %slice_bitcast_fusion = (bf16[16384,1,256]{0,2,1:T(8,128)(2,1)}, bf16[16384,256]{0,1:T(8,128)(2,1)}) fusion(bf16[16384,768]{0,1:T(8,128)(2,1)} %all-gather.2.cloned.1.call-done), kind=kLoop, calls=%fused_computation.49 | loop fusion | bytes 33554432 | tf_op jit(solution)/shard_map/reshape | solution.py:176
  207.6 11.9 %copy.177 = bf16[16384,1,2,128]{3,0,2,1:T(8,128)(2,1)} copy(bf16[16384,1,2,128]{0,3,2,1:T(8,128)(2,1)} %bitcast.232) | data formatting | bytes 16777216
  219.5 11.9 %copy.179 = bf16[16384,1,256]{2,0,1:T(8,128)(2,1)} copy(bf16[16384,1,256]{0,2,1:T(8,128)(2,1)} %get-tuple-element.497) | data formatting | bytes 16777216
  231.4 5.8 slice_bitcast_fusion.1
  237.2 6.4 copy.176
  245.8 26.8 %while.24 = (s32[]{:T(128)}, f32[1,4,2,256]{3,1,2,0:T(4,128)S(1)}, f32[1,4,2,256]{3,1,2,0:T(4,128)S(1)}, f32[1,4,2,256,128]{4,3,2,1,0:T(8,128)}, f32[1,2,2,256]{...) while((s32[]{:T(128)}, f32[1,4,2,256]{3,1,2,0:T(4,128)S(1)}, ...), condition=%wide.region_7.8_spmd.clone, body=%wide.region_0.7_spmd.clone.sunk | while | flops 1640245504 | bytes 62358088 | solution.py:217
  246.5 15.0 %conditional.3 = ((f32[1,4,2,256]{3,1,2,0:T(4,128)S(1)}, f32[1,4,2,256]{3,1,2,0:T(4,128)S(1)}, f32[1,4,2,256,128]{4,3,2,1,0:T(8,128)}, f32[1,2,2,256]{3,1,2,0:T(...) conditional(s32[]{:T(128)} %convert_element_type.160, (f32[1,4,2,256]{3,1,2,0:T(4,128)S(1)}, ...), branch_computations={%region_1.0_spmd, %region_2.6_spmd} | conditional | flops 1640245504 | bytes 62352608 | solution.py:214
  275.7 6.8 all_to_all.52
  284.6 3.9 all_to_all.53
  296.2 6.1 reshape.349
  302.3 285.5 %all_to_all.54 = bf16[64,12,2048]{2,1,0:T(8,128)(2,1)S(1)} all-to-all(bf16[64,12,2048]{2,1,0:T(8,128)(2,1)} %reshape.349), channel_id=1, replica_groups=mesh['sp'=64,'tp'=2] {'sp'}, dimensions={0} | all-to-all | bytes 6291456 | tf_op jit(solution)/shard_map/all_to_all | solution.py:252
  590.4 10.5 %all_to_all.55 = bf16[2,1,64,12,2048]{4,2,3,1,0:T(8,128)(2,1)S(1)} all-to-all(bf16[2,1,64,12,2048]{4,2,3,1,0:T(8,128)(2,1)S(1)} %broadcast_in_dim.87), channel_id=1, replica_groups=mesh['sp'=64,'tp'=2] {'tp'}, dimensions={0} | all-to-all | bytes 12582912 | tf_op jit(solution)/shard_map/all_to_all | solution.py:36
  607.7 10.1 %convolution_convert_fusion = bf16[2,128,6,2048]{3,1,2,0:T(8,128)(2,1)} fusion(bf16[2,256,2048]{2,1,0:T(8,128)(2,1)S(1)} %copy-done, f32[2,128,6,256]{3,1,2,0:T(8,128)} %fusion.47, bf16[128,2,6,2048]{3,0,2,1:T(8,128)(2,1)} %bitcast.235, bf16[2,2048,256]{2,1,0:T(8,128)(2,1)} %param.48), kind=kOutput, calls=%fused_computation.50 | convolution fusion | flops 3226730496 | bytes 18350080 | tf_op jit(solution)/shard_map/rjcf,jfd->rjcd/dot_general | solution.py:113
  621.2 10.0 %all_to_all.56 = bf16[2,1,64,12,2048]{4,2,3,1,0:T(8,128)(2,1)} all-to-all(bf16[2,1,64,12,2048]{4,2,3,1,0:T(8,128)(2,1)S(1)} %copy.196), channel_id=1, replica_groups=mesh['sp'=64,'tp'=2] {'tp'}, dimensions={0} | all-to-all | bytes 12582912 | tf_op jit(solution)/shard_map/all_to_all | solution.py:52
  631.2 7.0 reduce_sum.98
  638.1 5.7 copy.198
  643.8 6.1 all-to-all-start.5
  652.4 50.9 %all-to-all-done.5 = bf16[64,12,2048]{2,1,0:T(8,128)(2,1)} async-done(((bf16[64,12,2048]{2,1,0:T(8,128)(2,1)}), bf16[64,12,2048]{2,1,0:T(8,128)(2,1)}, u32[]{:S(2)}, u32[]{:S(2)}) %all-to-all-start.5) | async-done | bytes 3145760 | tf_op jit(solution)/shard_map/all_to_all | solution.py:263
  703.4 6.2 reshape.350
  709.5 7.6 %gather_fusion = bf16[512,2048]{1,0:T(8,128)(2,1)} fusion(bf16[768,2048]{1,0:T(8,128)(2,1)} %reshape.350, s32[1024]{0:T(1024)S(1)} %pad_clamp_fusion), kind=kCustom, calls=%fused_computation | custom fusion | bytes 4196352 | tf_op jit(solution)/shard_map/jit(_take)/gather | solution.py:267
  717.1 4.1 gather.7
  721.2 6.1 fusion.49
  727.3 4.7 multiply_reduce_fusion
  (176 shorter events, 57.5 us)
Async XLA Ops:
  6.5 601.2 %copy-start = (bf16[2,256,2048]{2,1,0:T(8,128)(2,1)S(1)}, bf16[2,256,2048]{2,1,0:T(8,128)(2,1)}, u32[]{:S(2)}) copy-start(bf16[2,256,2048]{2,1,0:T(8,128)(2,1)} %param.49) | copy-start | bytes 6291460
  6.5 9.8 %copy-start.11 = (s32[128,4]{0,1:T(4,128)S(1)}, s32[128,4]{0,1:T(4,128)}, u32[]{:S(2)}) copy-start(s32[128,4]{0,1:T(4,128)} %param.50) | copy-start | bytes 6148
  6.5 189.6 %all-gather.2.cloned.1.call-start = ((), (), s32[]{:S(2)}) async-start(), calls=%async_computation.6 | async-start | bytes 25559040 | tf_op jit(solution)/shard_map/all_gather | solution.py:25
  245.7 28.4 %copy-start.14 = (f32[2]{0:T(128)S(1)}, f32[2]{0:T(128)}, u32[]{:S(2)}) copy-start(f32[2]{0:T(128)} %param.35) | copy-start | bytes 28
  245.8 28.7 %copy-start.17 = (f32[256]{0:T(256)S(1)}, f32[256]{0:T(256)}, u32[]{:S(2)}) copy-start(f32[256]{0:T(256)} %param.37) | copy-start | bytes 3076
  248.6 1.2 copy-start.5
  251.9 1.0 copy-start.6
  255.3 2.4 copy-start.2
  260.5 1.0 copy-start.3
  272.6 10.8 %copy-start.4 = (f32[1,4,2,256,128]{4,3,2,1,0:T(8,128)S(1)}, f32[1,4,2,256,128]{4,3,2,1,0:T(8,128)}, u32[]{:S(2)}) copy-start(f32[1,4,2,256,128]{4,3,2,1,0:T(8,128)} %get-tuple-element.330) | copy-start | bytes 3145732
  272.6 11.1 %copy-start.15 = (f32[4]{0:T(128)S(1)}, f32[4]{0:T(128)}, u32[]{:S(2)}) copy-start(f32[4]{0:T(128)} %param.34) | copy-start | bytes 52
  274.2 9.9 %copy-start.18 = (f32[128]{0:T(128)S(1)}, f32[128]{0:T(128)}, u32[]{:S(2)}) copy-start(f32[128]{0:T(128)} %param.36) | copy-start | bytes 1540
  284.1 7.8 %copy-start.8 = (bf16[128,2,512]{0,2,1:T(8,128)(2,1)S(1)}, bf16[128,2,512]{0,2,1:T(8,128)(2,1)}, u32[]{:S(2)}) copy-start(bf16[128,2,512]{0,2,1:T(8,128)(2,1)} %copy.187) | copy-start | bytes 786436
  288.7 3.5 copy-start.7
  291.8 1.2 copy-start.9
  291.8 1.2 copy-start.12
  292.2 1.2 copy-start.10
  600.9 3.8 copy-start.19
  602.1 2.7 copy-start.1
  643.8 6.4 copy-start.16
  643.8 59.6 %all-to-all-start.5 = ((bf16[64,12,2048]{2,1,0:T(8,128)(2,1)}), bf16[64,12,2048]{2,1,0:T(8,128)(2,1)}, u32[]{:S(2)}, u32[]{:S(2)}) async-start(bf16[64,12,2048]{2,1,0:T(8,128)(2,1)} %copy.198), calls=%async_computation.5 | async-start | bytes 8388608 | tf_op jit(solution)/shard_map/all_to_all | solution.py:263
  727.3 4.7 copy-start.13
Sparse Core Ops, SparseCore 0:
  11.5 184.5 all-gather.1
where the time goes:
time: 756 us; the launch traced here: 742 us
  blocking collectives  317 us (42%)
  waiting for transfers between devices  230 us (30%)
  local copies, waits for them, and re-layouts  103 us (14%)
  matrix products  41.6 us (6%)
  other arithmetic  17.6 us (2%)
  between operations  14.3 us (2%)
  loops' own time  11.9 us (2%)
    all_to_all x1, blocking collectives, shards(): lax.all_to_all(outgoing, 'sp', split_axis=0, concat_axis=0, tiled=True)  285 us
    all_gather x1, waiting for transfers between devices, in_one_piece(): lax.all_gather(both, axis, axis=dim, tiled=True)  180 us
    all_to_all x1, waiting for transfers between devices, shards(): lax.all_to_all(own_sums[0].astype(jnp.bfloat16), 'sp', split_axis=0, conc...  50.9 us
    unnamed x46, local copies, waits for them, and re-layouts  40.6 us
  transfers between devices with their start and end apart: 2, of which 2 were waited for; matrix products, arithmetic and copies ran while one was open for 1% of the time, Pallas kernels for 0%

commit v1 on v0

v1 whole, which is shorter than its diff:
```python
import functools

import jax
import jax.numpy as jnp
import numpy as np
from jax import lax
from jax.experimental import pallas as pl
from jax.experimental.pallas import tpu as pltpu
from jax.sharding import PartitionSpec as P

D = 2048
TOPK = 4
EPS = 1e-06
TQ = 128
LOG2E = 1.4426950408889634
BK = 1024
RC = 256
CAP = 6
PIECES = 4
WIDTH = D // PIECES
SLAB = PIECES * CAP
EXPERTS = 128
GROUP = 16
GROUP_ROWS = GROUP * SLAB
VMEM_BYTES = 60 * 2**20
MESH = pl.DeviceIdType.MESH
ORDERS = ((0, 1, 2), (1, 2, 0), (2, 0, 1))
STRIDE = (1, 4, 16)

def gather_kernel(kv, out, lsem, ssem, rsem):
    sp = lax.axis_index("sp")
    tp = lax.axis_index("tp")
    at = (sp % 4, (sp // 4) % 4, sp // 16)

    def moved(d, by):
        return sp + ((at[d] + by) % 4 - at[d]) * STRIDE[d]

    def dev(d, by):
        return (moved(d, by), tp)

    barrier = pltpu.get_barrier_semaphore()
    for d in range(3):
        for by in (1, 3):
            pl.semaphore_signal(barrier, inc=1, device_id=dev(d, by), device_id_type=MESH)
    pl.semaphore_wait(barrier, 6)
    own = pltpu.make_async_copy(kv, out.at[at[2], at[1], at[0]], lsem)
    own.start()

    def region(c, p, shift, lo, n):
        order = ORDERS[c]
        idx = [at[0], at[1], at[2]]
        for d in order[:p]:
            idx[d] = slice(None)
        idx[order[p]] = (at[order[p]] + shift) % 4
        return out.at[idx[2], idx[1], idx[0], pl.ds(lo, n), pl.ds(256 * c, 256)]

    def send(c, p, k, src, dst, by):
        s = (c * 3 + p) * 4 + k
        return pltpu.make_async_remote_copy(src_ref=src, dst_ref=dst, send_sem=ssem.at[s], recv_sem=rsem.at[s],
                                            device_id=dev(ORDERS[c][p], by), device_id_type=MESH)
    sends = []
    for p in range(3):
        first = []
        for c in range(3):
            dst = region(c, p, 0, 0, 256)
            src = kv.at[:, pl.ds(256 * c, 256)] if p == 0 else dst
            a = send(c, p, 0, src, dst, 1)
            b = send(c, p, 1, src, dst, 3)
            a.start(); b.start()
            first.append((a, b))
        second = []
        for c in range(3):
            a, b = first[c]
            a.wait_recv()
            r = region(c, p, 3, 0, 128)
            fa = send(c, p, 2, r, r, 1)
            fa.start()
            b.wait_recv()
            r = region(c, p, 1, 128, 128)
            fb = send(c, p, 3, r, r, 3)
            fb.start()
            second.append((fa, fb))
        if p == 0:
            own.wait()
        for c in range(3):
            for f in second[c]:
                f.wait_recv()
        sends += first + second
    for a, b in sends:
        a.wait_send()
        b.wait_send()

def gather(kv):
    return pl.pallas_call(
        gather_kernel,
        in_specs=[pl.BlockSpec(memory_space=pltpu.VMEM)],
        out_specs=pl.BlockSpec(memory_space=pl.ANY),
        out_shape=jax.ShapeDtypeStruct((4, 4, 4, 256, 768), jnp.bfloat16),
        scratch_shapes=[pltpu.SemaphoreType.DMA, pltpu.SemaphoreType.DMA((36,)), pltpu.SemaphoreType.DMA((36,))],
        compiler_params=pltpu.CompilerParams(collective_id=3, has_side_effects=True),
        name="gather",
    )(kv)


def flash_kernel(sched, q_ref, kv_ref, lamn_ref, lamw_ref, gn_ref, gw_ref, o_ref, qn, qw, mn, mw, accn, accw, lw):
    s = pl.program_id(0)
    n_hi = sched[0]
    tile = (s >= n_hi).astype(jnp.int32)
    kb = s - tile * n_hi
    last = sched[0] * (1 - tile) + sched[1] * tile - 1
    base = sched[2 + tile]
    key0 = kb * BK

    @pl.when(kb == 0)
    def _():
        lane = lax.broadcasted_iota(jnp.int32, (TQ, 128), 1)
        z = jnp.zeros((TQ, 128), jnp.bfloat16)
        for h in range(4):
            qh = q_ref[0, :, h * 128:(h + 1) * 128]
            qn[h * TQ:(h + 1) * TQ, :] = jnp.where(lane < 64, qh, z)
            qn[(4 + h) * TQ:(5 + h) * TQ, :] = jnp.where(lane < 64, z, qh)
        for h in range(2):
            b = 512 + h * 256
            qw[h * TQ:(h + 1) * TQ, 0:128] = q_ref[0, :, b:b + 128]
            qw[h * TQ:(h + 1) * TQ, 128:256] = z
            qw[(2 + h) * TQ:(3 + h) * TQ, 0:128] = z
            qw[(2 + h) * TQ:(3 + h) * TQ, 128:256] = q_ref[0, :, b + 128:b + 256]
        mn[...] = jnp.full(mn.shape, -1e30, jnp.float32)
        mw[...] = jnp.full(mw.shape, -1e30, jnp.float32)
        accn[...] = jnp.zeros(accn.shape, jnp.float32)
        accw[...] = jnp.zeros(accw.shape, jnp.float32)
        lw[...] = jnp.zeros(lw.shape, jnp.float32)

    def step(masked):
        kn = kv_ref[:, 0:128]
        vn = jnp.concatenate([kv_ref[:, 128:256], jnp.ones((BK, 128), jnp.bfloat16)], axis=1)
        kw = kv_ref[:, 256:512]
        vw = kv_ref[:, 512:768]
        dn = (((1,), (1,)), ((), ()))
        chunks = [("n", r) for r in range(0, 8 * TQ, RC)] + [("w", r) for r in range(0, 4 * TQ, RC)]
        if masked:
            row = lax.broadcasted_iota(jnp.int32, (RC, BK), 0) & (TQ - 1)
            col = lax.broadcasted_iota(jnp.int32, (RC, BK), 1)
            keep = (col + key0) <= (row + base)

        def scores(c):
            kind, r = c
            if kind == "n":
                return lax.dot_general(qn[r:r + RC, :], kn, dn, preferred_element_type=jnp.float32)
            return lax.dot_general(qw[r:r + RC, :], kw, dn, preferred_element_type=jnp.float32)

        nxt = scores(chunks[0])
        for ci, c in enumerate(chunks):
            sc = nxt
            if ci + 1 < len(chunks):
                nxt = scores(chunks[ci + 1])
            kind, r = c
            m_ref = mn if kind == "n" else mw
            scale = (64 if kind == "n" else 128) ** -0.5 * LOG2E
            sc = sc * scale
            if masked:
                sc = jnp.where(keep, sc, -1e30)
            m_old = m_ref[r:r + RC, :]
            m_new = jnp.maximum(m_old, jnp.max(sc, axis=-1, keepdims=True))
            m_ref[r:r + RC, :] = m_new
            alpha = jnp.exp2(m_old - m_new)
            p = jnp.exp2(sc - jnp.tile(m_new, (1, BK // 128)))
            pb = p.astype(jnp.bfloat16)
            a2 = jnp.tile(alpha, (1, 2))
            if kind == "n":
                accn[r:r + RC, :] = accn[r:r + RC, :] * a2 + jnp.dot(pb, vn, preferred_element_type=jnp.float32)
            else:
                ps = p[:, 0:128]
                for j in range(1, BK // 128):
                    ps = ps + p[:, j * 128:(j + 1) * 128]
                lw[r:r + RC, :] = lw[r:r + RC, :] * alpha + ps
                accw[r:r + RC, :] = accw[r:r + RC, :] * a2 + jnp.dot(pb, vw, preferred_element_type=jnp.float32)

    @pl.when(kb < last)
    def _():
        step(False)

    @pl.when(kb == last)
    def _():
        step(True)
        for h in range(4):
            r0, r1 = h * TQ, (4 + h) * TQ
            d = accn[r0:r0 + TQ, 0:128] / accn[r0:r0 + TQ, 128:256] - lamn_ref[h] * (accn[r1:r1 + TQ, 0:128] / accn[r1:r1 + TQ, 128:256])
            d = d * lax.rsqrt(jnp.mean(d * d, axis=-1, keepdims=True) + EPS) * gn_ref[...]
            o_ref[0, :, h * 128:(h + 1) * 128] = d.astype(jnp.bfloat16)
        for h in range(2):
            r0, r1 = h * TQ, (2 + h) * TQ
            l0 = jnp.sum(lw[r0:r0 + TQ, :], axis=-1, keepdims=True)
            l1 = jnp.sum(lw[r1:r1 + TQ, :], axis=-1, keepdims=True)
            d = accw[r0:r0 + TQ, :] / l0 - lamw_ref[h] * (accw[r1:r1 + TQ, :] / l1)
            d = d * lax.rsqrt(jnp.mean(d * d, axis=-1, keepdims=True) + EPS) * gw_ref[...]
            o_ref[0, :, 512 + h * 256:512 + (h + 1) * 256] = d.astype(jnp.bfloat16)


def flash(sched, q, kv, lamn, lamw, gn, gw):
    steps = (kv.shape[0] // 256 + BK // 256) // (BK // 256)
    def tile_of(s, sc):
        return (s >= sc[0]).astype(jnp.int32)
    gs = pltpu.PrefetchScalarGridSpec(
        num_scalar_prefetch=1, grid=(steps,),
        in_specs=[
            pl.BlockSpec((1, TQ, 1024), lambda s, sc: (tile_of(s, sc), 0, 0)),
            pl.BlockSpec((BK, 768), lambda s, sc: (s - tile_of(s, sc) * sc[0], 0)),
            pl.BlockSpec(memory_space=pltpu.SMEM),
            pl.BlockSpec(memory_space=pltpu.SMEM),
            pl.BlockSpec((1, 128), lambda s, sc: (0, 0)),
            pl.BlockSpec((1, 256), lambda s, sc: (0, 0)),
        ],
        out_specs=pl.BlockSpec((1, TQ, 1024), lambda s, sc: (tile_of(s, sc), 0, 0)),
        scratch_shapes=[
            pltpu.VMEM((8 * TQ, 128), jnp.bfloat16), pltpu.VMEM((4 * TQ, 256), jnp.bfloat16),
            pltpu.VMEM((8 * TQ, 128), jnp.float32), pltpu.VMEM((4 * TQ, 128), jnp.float32),
            pltpu.VMEM((8 * TQ, 256), jnp.float32), pltpu.VMEM((4 * TQ, 256), jnp.float32),
            pltpu.VMEM((4 * TQ, 128), jnp.float32),
        ])
    return pl.pallas_call(
        flash_kernel, grid_spec=gs,
        out_shape=jax.ShapeDtypeStruct((2, TQ, 1024), jnp.bfloat16),
        compiler_params=pltpu.CompilerParams(dimension_semantics=("arbitrary",), vmem_limit_bytes=VMEM_BYTES),
        name="flash",
    )(sched, q, kv, lamn, lamw, gn.reshape(1, 128), gw.reshape(1, 256))

def sched_of(i, n_blocks):
    a = jnp.minimum(i, n_blocks - 1 - i); b = n_blocks - 1 - a
    h = (i >= n_blocks // 2).astype(jnp.int32)
    w = BK // 256
    return jnp.stack([(b + w) // w, (a + w) // w, b * 256 + h * 128, a * 256 + h * 128]).astype(jnp.int32)


def rms(v, gain):
    return v * lax.rsqrt(jnp.mean(v * v, axis=-1, keepdims=True) + EPS) * gain


def dot(a, b):
    return jnp.dot(a, b, preferred_element_type=jnp.float32)


def ranks(ids):
    lane = lax.broadcasted_iota(jnp.int32, (TQ, EXPERTS), 1)
    named = jnp.zeros((TQ, EXPERTS), jnp.float32)
    for k in range(TOPK):
        named = named + (ids[:, k : k + 1] == lane).astype(jnp.float32)
    below = lax.broadcasted_iota(jnp.int32, (TQ, TQ), 1) < lax.broadcasted_iota(
        jnp.int32, (TQ, TQ), 0
    )
    count = dot(below.astype(jnp.bfloat16), named.astype(jnp.bfloat16))
    return (named * (count + 1.0)).astype(jnp.bfloat16)


def mid_kernel(
    f0, f1, on, ow, stream, gmix, gffn, ids, rank_of, piece_mask, mixed_out, normed_out, slab
):
    projected = (
        dot(f0[:, 0:512], on[0:512, :])
        + dot(f1[:, 0:512], on[512:1024, :])
        + dot(f0[:, 512:1024], ow[0:512, :])
        + dot(f1[:, 512:1024], ow[512:1024, :])
    )
    mixed = (stream[...].astype(jnp.float32) + rms(projected, gmix[...])).astype(jnp.bfloat16)
    mixed_out[...] = mixed
    normed = rms(mixed.astype(jnp.float32), gffn[...]).astype(jnp.bfloat16)
    normed_out[...] = normed
    stacked = jnp.concatenate([normed[:, c * WIDTH : (c + 1) * WIDTH] for c in range(PIECES)], 0)
    value = ranks(ids[...])
    row = lax.broadcasted_iota(jnp.int32, (GROUP_ROWS, EXPERTS), 0)
    lane = lax.broadcasted_iota(jnp.int32, (GROUP_ROWS, EXPERTS), 1)
    for g in range(EXPERTS // GROUP):
        low = (lane - g * GROUP) * SLAB
        spread = ((row >= low) & (row < low + SLAB)).astype(jnp.bfloat16)
        here = lax.dot_general(
            spread, value, (((1,), (1,)), ((), ())), preferred_element_type=jnp.float32
        )
        chosen = (here == rank_of[...]).astype(jnp.float32).astype(jnp.bfloat16)
        chosen = jnp.concatenate([chosen] * PIECES, axis=1) * piece_mask[...]
        slab[g * GROUP_ROWS : (g + 1) * GROUP_ROWS, :] = dot(chosen, stacked).astype(jnp.bfloat16)


def slab_tables():
    i = np.arange(GROUP_ROWS) % SLAB
    rank = np.broadcast_to((i % CAP + 1)[:, None], (GROUP_ROWS, EXPERTS)).astype(np.float32)
    piece = (i // CAP)[:, None] == (np.arange(PIECES * TQ) // TQ)[None, :]
    return rank, piece.astype(np.float32)


def order_table():
    i = np.arange(GROUP_ROWS)
    to = (i % SLAB // CAP) * (GROUP * CAP) + (i // SLAB) * CAP + i % CAP
    table = np.zeros((GROUP_ROWS, GROUP_ROWS), np.float32)
    table[to, i] = 1.0
    return table


def mid(f0, f1, on, ow, stream, gmix, gffn, ids):
    rank, piece = slab_tables()
    return pl.pallas_call(
        mid_kernel,
        out_shape=(
            jax.ShapeDtypeStruct((TQ, D), jnp.bfloat16),
            jax.ShapeDtypeStruct((TQ, D), jnp.bfloat16),
            jax.ShapeDtypeStruct((EXPERTS * SLAB, WIDTH), jnp.bfloat16),
        ),
        compiler_params=pltpu.CompilerParams(vmem_limit_bytes=VMEM_BYTES),
        cost_estimate=pl.CostEstimate(flops=4 * 10**9, bytes_accessed=14 * 10**6, transcendentals=0),
        name="mid",
    )(
        f0,
        f1,
        on,
        ow,
        stream,
        gmix.reshape(1, D),
        gffn.reshape(1, D),
        ids,
        jnp.asarray(rank),
        jnp.asarray(piece, jnp.bfloat16),
    )


def expert_kernel(x, g1, u1, d1, g2, u2, d2, order, order_t, out, rows, results):
    span = GROUP * CAP
    for g in range(EXPERTS // GROUP):
        got = dot(order[...], x[g * GROUP_ROWS : (g + 1) * GROUP_ROWS, :]).astype(jnp.bfloat16)
        for c in range(PIECES):
            rows[g * span : (g + 1) * span, c * WIDTH : (c + 1) * WIDTH] = got[
                c * span : (c + 1) * span, :
            ]
    for m in range(0, EXPERTS * CAP, 256):
        part = rows[m : m + 256, :]
        total = None
        for gate, up, down in ((g1, u1, d1), (g2, u2, d2)):
            gated = dot(part, gate[0])
            hidden = (gated / (1.0 + jnp.exp(-gated)) * dot(part, up[0])).astype(jnp.bfloat16)
            term = dot(hidden, down[0])
            total = term if total is None else total + term
        results[m : m + 256, :] = total.astype(jnp.bfloat16)
    for g in range(EXPERTS // GROUP):
        stacked = jnp.concatenate(
            [
                results[g * span : (g + 1) * span, c * WIDTH : (c + 1) * WIDTH]
                for c in range(PIECES)
            ],
            0,
        )
        out[g * GROUP_ROWS : (g + 1) * GROUP_ROWS, :] = dot(order_t[...], stacked).astype(
            jnp.bfloat16
        )


def run_expert(which, x, gate, up, down, gate2, up2, down2):
    table = order_table()
    full = lambda *shape: pl.BlockSpec(shape, lambda i, w: (0,) * len(shape))
    mine = lambda *shape: pl.BlockSpec((1, *shape), lambda i, w: (w[0], 0, 0))
    half = gate.shape[2]
    return pl.pallas_call(
        expert_kernel_with_prefetch,
        grid_spec=pltpu.PrefetchScalarGridSpec(
            num_scalar_prefetch=1,
            grid=(1,),
            in_specs=[
                full(EXPERTS * SLAB, WIDTH),
                mine(D, half),
                mine(D, half),
                mine(half, D),
                full(1, D, half),
                full(1, D, half),
                full(1, half, D),
                full(GROUP_ROWS, GROUP_ROWS),
                full(GROUP_ROWS, GROUP_ROWS),
            ],
            out_specs=full(EXPERTS * SLAB, WIDTH),
            scratch_shapes=[
                pltpu.VMEM((EXPERTS * CAP, D), jnp.bfloat16),
                pltpu.VMEM((EXPERTS * CAP, D), jnp.bfloat16),
            ],
        ),
        out_shape=jax.ShapeDtypeStruct((EXPERTS * SLAB, WIDTH), jnp.bfloat16),
        compiler_params=pltpu.CompilerParams(vmem_limit_bytes=VMEM_BYTES),
        cost_estimate=pl.CostEstimate(flops=6 * 10**9, bytes_accessed=14 * 10**6, transcendentals=0),
        name="expert",
    )(
        which,
        x,
        gate,
        up,
        down,
        gate2,
        up2,
        down2,
        jnp.asarray(table, jnp.bfloat16),
        jnp.asarray(table.T, jnp.bfloat16),
    )


def expert_kernel_with_prefetch(which, *refs):
    expert_kernel(*refs)


def combine_kernel(back, ids, weights, shared, mixed, gpost, rank_row, piece_row, out):
    value = ranks(ids[...])
    lane = lax.broadcasted_iota(jnp.int32, (TQ, EXPERTS), 1)
    share = jnp.zeros((TQ, EXPERTS), jnp.float32)
    for k in range(TOPK):
        share = share + jnp.where(ids[:, k : k + 1] == lane, weights[:, k : k + 1], 0.0)
    share = share.astype(jnp.bfloat16)
    row = lax.broadcasted_iota(jnp.int32, (EXPERTS, GROUP_ROWS), 0)
    col = lax.broadcasted_iota(jnp.int32, (EXPERTS, GROUP_ROWS), 1)
    total = jnp.zeros((PIECES * TQ, WIDTH), jnp.float32)
    for g in range(EXPERTS // GROUP):
        low = (row - g * GROUP) * SLAB
        spread = ((col >= low) & (col < low + SLAB)).astype(jnp.bfloat16)
        held = jnp.where(dot(value, spread) == rank_row[...], dot(share, spread), 0.0)
        picks = jnp.concatenate(
            [jnp.where(piece_row[...] == float(c), held, 0.0) for c in range(PIECES)], 0
        ).astype(jnp.bfloat16)
        total = total + dot(picks, back[g * GROUP_ROWS : (g + 1) * GROUP_ROWS, :])
    routed = jnp.concatenate([total[c * TQ : (c + 1) * TQ, :] for c in range(PIECES)], axis=1)
    combined = shared[...] + routed
    out[...] = (mixed[...].astype(jnp.float32) + rms(combined, gpost[...])).astype(jnp.bfloat16)


def combine(back, ids, weights, shared, mixed, gpost):
    i = np.arange(GROUP_ROWS) % SLAB
    return pl.pallas_call(
        combine_kernel,
        out_shape=jax.ShapeDtypeStruct((TQ, D), jnp.bfloat16),
        compiler_params=pltpu.CompilerParams(vmem_limit_bytes=VMEM_BYTES),
        cost_estimate=pl.CostEstimate(flops=3 * 10**9, bytes_accessed=6 * 10**6, transcendentals=0),
        name="combine",
    )(
        back,
        ids,
        weights,
        shared,
        mixed,
        gpost.reshape(1, D),
        jnp.asarray((i % CAP + 1)[None, :], jnp.float32),
        jnp.asarray((i // CAP)[None, :], jnp.float32),
    )


BOTH = ("sp", "tp")


def exchanged(slab):
    pieces = slab.reshape(EXPERTS, SLAB, WIDTH)
    return lax.all_to_all(pieces, BOTH, 0, 0, tiled=True).reshape(EXPERTS * SLAB, WIDTH)


def shards(
    queries_narrow,
    keys_narrow,
    values_narrow,
    queries_wide,
    keys_wide,
    values_wide,
    lambda_narrow,
    lambda_wide,
    gain_narrow,
    gain_wide,
    out_narrow,
    out_wide,
    stream,
    gain_mix,
    gain_ffn,
    gain_post,
    shared_gate,
    shared_up,
    shared_down,
    expert_gate,
    expert_up,
    expert_down,
    expert_ids,
    route_weights,
):
    sp = lax.axis_index("sp")
    tp = lax.axis_index("tp")
    n_sp = lax.axis_size("sp")
    late = sp >= n_sp // 2
    half = late.astype(jnp.int32)

    kv = jnp.concatenate([keys_narrow, values_narrow, keys_wide, values_wide], axis=1)
    queries = jnp.concatenate([queries_narrow, queries_wide], axis=1)
    mirror = [(i, n_sp - 1 - i) for i in range(n_sp)]
    kept = lax.dynamic_slice_in_dim(queries, half * TQ, TQ, 0)
    given = lax.dynamic_slice_in_dim(queries, (1 - half) * TQ, TQ, 0)
    taken = lax.ppermute(given, "sp", mirror)
    tiles = jnp.stack([jnp.where(late, kept, taken), jnp.where(late, taken, kept)])
    across = [(0, 1), (1, 0)]
    other = [
        lax.ppermute(lax.dynamic_slice_in_dim(w, 1 - tp, 1, 0), "tp", across)
        for w in (expert_gate, expert_up, expert_down)
    ]
    gathered = gather(kv).reshape(n_sp * 2 * TQ, kv.shape[1])
    attended = flash(
        sched_of(sp, n_sp), tiles, gathered, lambda_narrow, lambda_wide, gain_narrow, gain_wide
    )
    own = jnp.where(late, attended[0], attended[1])
    away = jnp.where(late, attended[1], attended[0])
    first, second = [], []
    for i in range(n_sp):
        h = int(i >= n_sp // 2)
        home, abroad = 2 * i + h, 2 * (n_sp - 1 - i) + h
        first += [(2 * i, home), (2 * i + 1, abroad)]
        second += [(2 * i, abroad), (2 * i + 1, home)]
    a = lax.ppermute(jnp.where(tp == 0, own, away), BOTH, first)
    b = lax.ppermute(jnp.where(tp == 0, away, own), BOTH, second)
    f0 = jnp.where(tp == half, a, b)
    f1 = jnp.where(tp == half, b, a)
    mixed, normed, slab = mid(
        f0, f1, out_narrow, out_wide, stream, gain_mix, gain_ffn, expert_ids
    )
    incoming = exchanged(slab)
    results = run_expert(
        jnp.reshape(tp, (1,)).astype(jnp.int32),
        incoming,
        expert_gate,
        expert_up,
        expert_down,
        *other,
    )
    back = exchanged(results)
    shared_hidden = (
        jax.nn.silu(dot(normed, shared_gate)) * dot(normed, shared_up)
    ).astype(jnp.bfloat16)
    shared_out = dot(shared_hidden, shared_down)
    return combine(back, expert_ids, route_weights, shared_out, mixed, gain_post)


def solution(mesh):
    return jax.shard_map(
        shards,
        mesh=mesh,
        in_specs=(
            P("sp", "tp"),
            P("sp", "tp"),
            P("sp", "tp"),
            P("sp", "tp"),
            P("sp", "tp"),
            P("sp", "tp"),
            P("tp"),
            P("tp"),
            P(),
            P(),
            P(),
            P(),
            P(("sp", "tp"), None),
            P(),
            P(),
            P(),
            P(),
            P(),
            P(),
            P("sp", None, "tp"),
            P("sp", None, "tp"),
            P("sp", "tp", None),
            P(("sp", "tp"), None),
            P(("sp", "tp"), None),
        ),
        out_specs=P(("sp", "tp"), None),
        check_vma=False,
    )
```

time: 756 us -> 310 us (0.41); the launches traced: 742 us -> 309 us
  blocking collectives: 317 us -> 0 us
  Pallas kernels: 0 us -> 178 us
  waiting for transfers between devices: 230 us -> 81.8 us
  local copies, waits for them, and re-layouts: 103 us -> 6.29 us
  matrix products: 41.6 us -> 5.44 us
  starting transfers between devices: 6.06 us -> 32.6 us
  between operations: 14.3 us -> 0.17 us
  other arithmetic: 17.6 us -> 5.31 us
  loops' own time: 11.9 us -> 0 us
    all_to_all x5 -> x0, blocking collectives: 317 us -> none  [the longest x1 285 us: shards(): lax.all_to_all(outgoing, 'sp', split_axis=0, concat_axis=0, tiled=True)]
    all_gather x1 -> x0, waiting for transfers between devices: 180 us -> none  [in_one_piece(): lax.all_gather(both, axis, axis=dim, tiled=True)]
    pallas_call x0 -> x5, Pallas kernels: none -> 178 us  [the longest x1 101 us: gather(): pl.pallas_call(gather_kernel, in_specs=[pl.BlockSpec(memory_space=pltpu.V...]
    unnamed x46 -> x19, local copies, waits for them, and re-layouts: 40.6 us -> 3.67 us
    dot_general x12 -> x2, matrix products: 41.6 us -> 5.44 us  [dot(): return jnp.dot(a, b, preferred_element_type=jnp.float32)]
    reshape x5 -> x0, local copies, waits for them, and re-layouts: 29.6 us -> none  [the longest x1 11.5 us: shards(): wide_values = pieces[3].reshape(key_count, wide_groups, VW)]
    ppermute x0 -> x6, starting transfers between devices: none -> 22.1 us  [the longest x1 9.32 us: shards(): a = lax.ppermute(jnp.where(tp == 0, own, away), BOTH, first)]
    all_to_all x1 -> x2, waiting for transfers between devices: 50.9 us -> 68.2 us  [exchanged(): lax.all_to_all(pieces, BOTH, 0, 0, tiled=True)]
  transfers between devices with their start and end apart: 2 -> 8, of which waited for: 2 -> 7; matrix products, arithmetic and copies ran while one was open for 1% -> 4% of each run, Pallas kernels for 0% -> 33%
where the time goes in v1:
time: 310 us; the launch traced here: 309 us
  Pallas kernels  178 us (57%)
  waiting for transfers between devices  81.8 us (26%)
  starting transfers between devices  32.6 us (11%)
  local copies, waits for them, and re-layouts  6.29 us (2%)
  matrix products  5.44 us (2%)
  other arithmetic  5.31 us (2%)
    pallas_call x1, Pallas kernels, gather(): pl.pallas_call(gather_kernel, in_specs=[pl.BlockSpec(memory_space=pltpu.V...  101 us
    all_to_all x2, waiting for transfers between devices, exchanged(): lax.all_to_all(pieces, BOTH, 0, 0, tiled=True)  68.2 us
    pallas_call x1, Pallas kernels, flash(): pl.pallas_call(flash_kernel, grid_spec=gs, out_shape=jax.ShapeDtypeStruct...  45 us
    pallas_call x1, Pallas kernels, run_expert(): pl.pallas_call(expert_kernel_with_prefetch, grid_spec=pltpu.PrefetchScala...  14.2 us
    all_to_all x2, starting transfers between devices, exchanged(): lax.all_to_all(pieces, BOTH, 0, 0, tiled=True)  10.4 us
    pallas_call x1, Pallas kernels, mid(): pl.pallas_call(mid_kernel, out_shape=(jax.ShapeDtypeStruct((TQ, D), jnp.b...  10 us
    ppermute x1, waiting for transfers between devices, shards(): b = lax.ppermute(jnp.where(tp == 0, away, own), BOTH, second)  9.52 us
    ppermute x1, starting transfers between devices, shards(): a = lax.ppermute(jnp.where(tp == 0, own, away), BOTH, first)  9.32 us
  transfers between devices with their start and end apart: 8, of which 7 were waited for; matrix products, arithmetic and copies ran while one was open for 4% of the time, Pallas kernels for 33%

profile of v1, /device:TPU:1, one launch (start us, length us, event | category | flops | bytes accessed | tf_op | source)
XLA Modules:
  0.0 309.4 jit_solution(483756428386643645)
XLA Ops:
  0.0 1.1 constant_dynamic-update-slice_fusion.1
  1.1 1.0 constant_dynamic-update-slice_fusion
  2.2 9.3 %collective-permute-start = (bf16[128,1024]{1,0:T(8,128)(2,1)S(1)}, bf16[128,1024]{1,0:T(8,128)(2,1)S(1)}, u32[]{:S(2)}, u32[]{:S(2)}) collective-permute-start(bf16[128,1024]{1,0:T(8,128)(2,1)S(1)} %constant_dynamic-slice_fusion.3), channel_id=1, source_target_pairs={{0,126},{2,124},{4,122},{6,120},{8,118},{10,116},{12,114},{14,112}... | collective-permute-start | bytes 786440 | tf_op jit(solution)/shard_map/ppermute | solution.py:491
  11.5 1.8 pad_maximum_fusion.1.kv
  13.2 101.4 %gather.1 = bf16[4,4,4,256,768]{4,3,2,1,0:T(8,128)(2,1)} custom-call(bf16[256,768]{1,0:T(8,128)(2,1)} %pad_maximum_fusion.1.kv), custom_call_target="tpu_custom_call" | custom-call | tf_op jit(solution)/shard_map/gather/pallas_call | solution.py:94
  116.3 45.0 %flash.1 = bf16[2,128,1024]{2,1,0:T(8,128)(2,1)} custom-call(s32[4]{0:T(128)} %pad_add_fusion.sched, bf16[2,128,1024]{2,1,0:T(8,128)(2,1)} %pad_maximum_fusion.q_ref, bf16[16384,768]{1,0:T(8,128)(2,1)} %bitcast.28, f32[4]{0:T(128)} %lamn_ref.1, f32[2]{0:T(128)} %lamw_ref.1, f32[1,128]{1,0:T(1,128)} %bitcast.32, f32[1,256]{1,0:T(1,128)} %bitcast.31), custom_call_target="tpu_custom_call" | custom-call | tf_op jit(solution)/shard_map/flash/pallas_call | solution.py:221
  161.3 1.1 select_bitcast_fusion
  162.4 9.3 %collective-permute-start.1 = (bf16[128,1024]{1,0:T(8,128)(2,1)S(1)}, bf16[128,1024]{1,0:T(8,128)(2,1)S(1)}, u32[]{:S(2)}, u32[]{:S(2)}) collective-permute-start(bf16[128,1024]{1,0:T(8,128)(2,1)S(1)} %get-tuple-element.16), channel_id=1, source_target_pairs={{0,0},{1,126},{2,2},{3,124},{4,4},{5,122},{6,6},{7,120},{8,8},{9,1... | collective-permute-start | bytes 786440 | tf_op jit(solution)/shard_map/ppermute | solution.py:510
  171.7 1.9 collective-permute-start.2
  174.4 0.9 collective-permute-done.1
  175.3 9.5 %collective-permute-done.2 = bf16[128,1024]{1,0:T(8,128)(2,1)S(1)} collective-permute-done((bf16[128,1024]{1,0:T(8,128)(2,1)S(1)}, bf16[128,1024]{1,0:T(8,128)(2,1)S(1)}, u32[]{:S(2)}, u32[]{:S(2)}) %collective-permute-start.2) | collective-permute-done | bytes 262176 | tf_op jit(solution)/shard_map/ppermute | solution.py:511
  185.7 10.0 %mid.1 = (bf16[128,2048]{1,0:T(8,128)(2,1)}, bf16[128,2048]{1,0:T(8,128)(2,1)}, bf16[3072,512]{1,0:T(8,128)(2,1)}) custom-call(bf16[128,1024]{1,0:T(8,128)(2,1)} %get-tuple-element.14.f0, bf16[128,1024]{1,0:T(8,128)(2,1)} %get-tuple-element.13.f1, bf16[1024,2048]{1,0:T(8,128)(2,1)} %on.1, bf16[1024,2048]{1,0:T(8,128)(2,1)} %ow.1, bf16[128,2048]{1,0:T(8,128)(2,1)} %stream.1, ...), custom_call_target="tpu_custom_call" | custom-call | flops 4000000000 | bytes 14000000 | tf_op jit(solution)/shard_map/mid/pallas_call | solution.py:300
  195.7 4.7 %all-to-all-start = ((bf16[128,24,512]{2,1,0:T(8,128)(2,1)}), bf16[128,24,512]{2,1,0:T(8,128)(2,1)}, u32[]{:S(2)}, u32[]{:S(2)}) async-start(bf16[128,24,512]{2,1,0:T(8,128)(2,1)} %bitcast.29), calls=%async_computation | async-start | bytes 6291456 | tf_op jit(solution)/shard_map/all_to_all | solution.py:451
  200.4 1.4 constant_dynamic-slice_fusion.2
  203.6 1.1 collective-permute-done.3.refs_4_
  204.7 1.5 collective-permute-done.4.refs_5_
  206.2 1.1 copy-done.7
  207.9 33.1 %all-to-all-done = bf16[128,24,512]{2,1,0:T(8,128)(2,1)} async-done(((bf16[128,24,512]{2,1,0:T(8,128)(2,1)}), bf16[128,24,512]{2,1,0:T(8,128)(2,1)}, u32[]{:S(2)}, u32[]{:S(2)}) %all-to-all-start) | async-done | bytes 3145760 | tf_op jit(solution)/shard_map/all_to_all | solution.py:451
  240.9 14.2 %expert.1 = bf16[3072,512]{1,0:T(8,128)(2,1)} custom-call(s32[1]{0:T(128)} %bitcast.which, bf16[3072,512]{1,0:T(8,128)(2,1)} %bitcast.15.refs_0_, bf16[2,2048,256]{2,1,0:T(8,128)(2,1)} %refs_1_.1, bf16[2,2048,256]{2,1,0:T(8,128)(2,1)} %refs_2_.1, bf16[2,256,2048]{2,1,0:T(8,128)(2,1)} %refs_3_.1, bf16[1,2048,256]{2,1,0:T(8,128)(2,1)} %copy-done.6, ...), custom_call_target="tpu_custom_call" | custom-call | flops 6000000000 | bytes 14000000 | tf_op jit(solution)/shard_map/expert/pallas_call | solution.py:359
  255.1 5.8 %all-to-all-start.1 = ((bf16[128,24,512]{2,1,0:T(8,128)(2,1)}), bf16[128,24,512]{2,1,0:T(8,128)(2,1)}, u32[]{:S(2)}, u32[]{:S(2)}) async-start(bf16[128,24,512]{2,1,0:T(8,128)(2,1)} %bitcast.30), calls=%async_computation.1 | async-start | bytes 6291456 | tf_op jit(solution)/shard_map/all_to_all | solution.py:451
  261.6 2.0 fusion.5
  263.7 3.4 %fusion.shared = f32[128,2048]{1,0:T(8,128)} fusion(bf16[512,2048]{1,0:T(8,128)(2,1)S(1)} %copy-done, f32[128,512]{1,0:T(8,128)S(1)} %fusion.5, bf16[128,2048]{1,0:T(8,128)(2,1)S(1)} %copy-done.1, bf16[2048,512]{1,0:T(8,128)(2,1)} %param.47), kind=kOutput, calls=%fused_computation.11 | convolution fusion | flops 537264128 | bytes 6029312 | tf_op jit(solution)/shard_map/dot_general | solution.py:240
  267.1 35.1 %all-to-all-done.1 = bf16[128,24,512]{2,1,0:T(8,128)(2,1)} async-done(((bf16[128,24,512]{2,1,0:T(8,128)(2,1)}), bf16[128,24,512]{2,1,0:T(8,128)(2,1)}, u32[]{:S(2)}, u32[]{:S(2)}) %all-to-all-start.1) | async-done | bytes 3145760 | tf_op jit(solution)/shard_map/all_to_all | solution.py:451
  302.2 7.2 %combine.1 = bf16[128,2048]{1,0:T(8,128)(2,1)} custom-call(bf16[3072,512]{1,0:T(8,128)(2,1)} %bitcast.17.back, s32[128,4]{1,0:T(8,128)} %copy.31.ids, f32[128,4]{1,0:T(8,128)} %copy.33.weights, f32[128,2048]{1,0:T(8,128)} %fusion.shared, bf16[128,2048]{1,0:T(8,128)(2,1)} %get-tuple-element.10.mixed, f32[1,2048]{1,0:T(1,128)} %bitcast.35, ...), custom_call_target="tpu_custom_call" | custom-call | flops 3000000000 | bytes 6000000 | tf_op jit(solution)/shard_map/combine/pallas_call | solution.py:428
  (29 shorter events, 6.3 us)
Async XLA Ops:
  0.0 263.7 %copy-start = (bf16[512,2048]{1,0:T(8,128)(2,1)S(1)}, bf16[512,2048]{1,0:T(8,128)(2,1)}, u32[]{:S(2)}) copy-start(bf16[512,2048]{1,0:T(8,128)(2,1)} %param.48) | copy-start | bytes 6291460
  2.2 113.1 %collective-permute-start = (bf16[128,1024]{1,0:T(8,128)(2,1)S(1)}, bf16[128,1024]{1,0:T(8,128)(2,1)S(1)}, u32[]{:S(2)}, u32[]{:S(2)}) collective-permute-start(bf16[128,1024]{1,0:T(8,128)(2,1)S(1)} %constant_dynamic-slice_fusion.3), channel_id=1, source_target_pairs={{0,126},{2,124},{4,122},{6,120},{8,118},{10,116},{12,114},{14,112}... | collective-permute-start | bytes 786440 | tf_op jit(solution)/shard_map/ppermute | solution.py:491
  116.3 57.4 %copy-start.4 = (s32[128,4]{0,1:T(4,128)S(1)}, s32[128,4]{0,1:T(4,128)}, u32[]{:S(2)}) copy-start(s32[128,4]{0,1:T(4,128)} %param.52) | copy-start | bytes 6148
  162.4 12.9 %collective-permute-start.1 = (bf16[128,1024]{1,0:T(8,128)(2,1)S(1)}, bf16[128,1024]{1,0:T(8,128)(2,1)S(1)}, u32[]{:S(2)}, u32[]{:S(2)}) collective-permute-start(bf16[128,1024]{1,0:T(8,128)(2,1)S(1)} %get-tuple-element.16), channel_id=1, source_target_pairs={{0,0},{1,126},{2,2},{3,124},{4,4},{5,122},{6,6},{7,120},{8,8},{9,1... | collective-permute-start | bytes 786440 | tf_op jit(solution)/shard_map/ppermute | solution.py:510
  171.7 13.1 %collective-permute-start.2 = (bf16[128,1024]{1,0:T(8,128)(2,1)S(1)}, bf16[128,1024]{1,0:T(8,128)(2,1)S(1)}, u32[]{:S(2)}, u32[]{:S(2)}) collective-permute-start(bf16[128,1024]{1,0:T(8,128)(2,1)S(1)} %get-tuple-element.15), channel_id=1, source_target_pairs={{0,126},{1,0},{2,124},{3,2},{4,122},{5,4},{6,120},{7,6},{8,118},{9... | collective-permute-start | bytes 786440 | tf_op jit(solution)/shard_map/ppermute | solution.py:511
  195.7 45.2 %all-to-all-start = ((bf16[128,24,512]{2,1,0:T(8,128)(2,1)}), bf16[128,24,512]{2,1,0:T(8,128)(2,1)}, u32[]{:S(2)}, u32[]{:S(2)}) async-start(bf16[128,24,512]{2,1,0:T(8,128)(2,1)} %bitcast.29), calls=%async_computation | async-start | bytes 6291456 | tf_op jit(solution)/shard_map/all_to_all | solution.py:451
  200.4 2.1 copy-start.2
  200.4 2.8 copy-start.3
  201.8 2.9 collective-permute-start.3
  202.5 3.7 %collective-permute-start.4 = (bf16[1,2048,256]{2,1,0:T(8,128)(2,1)S(1)}, bf16[1,2048,256]{2,1,0:T(8,128)(2,1)S(1)}, u32[]{:S(2)}, u32[]{:S(2)}) collective-permute-start(bf16[1,2048,256]{2,1,0:T(8,128)(2,1)S(1)} %constant_dynamic-slice_fusion.1), channel_id=1, source_target_pairs={{0,1},{1,0},{2,3},{3,2},{4,5},{5,4},{6,7},{7,6},{8,9},{9,8},{10,11... | collective-permute-start | bytes 3145736 | tf_op jit(solution)/shard_map/ppermute | solution.py:495
  203.2 4.6 %collective-permute-start.5 = (bf16[1,256,2048]{2,1,0:T(8,128)(2,1)S(1)}, bf16[1,256,2048]{2,1,0:T(8,128)(2,1)}, u32[]{:S(2)}, u32[]{:S(2)}) collective-permute-start(bf16[1,256,2048]{2,1,0:T(8,128)(2,1)S(1)} %constant_dynamic-slice_fusion), channel_id=1, source_target_pairs={{0,1},{1,0},{2,3},{3,2},{4,5},{5,4},{6,7},{7,6},{8,9},{9,8},{10,11... | collective-permute-start | bytes 3145736 | tf_op jit(solution)/shard_map/ppermute | solution.py:495
  204.7 36.2 %copy-start.6 = (bf16[1,2048,256]{2,1,0:T(8,128)(2,1)}, bf16[1,2048,256]{2,1,0:T(8,128)(2,1)S(1)}, u32[]{:S(2)}) copy-start(bf16[1,2048,256]{2,1,0:T(8,128)(2,1)S(1)} %collective-permute-done.3.refs_4_) | copy-start | bytes 3145732
  206.2 1.1 copy-start.7
  255.1 5.8 %copy-start.5 = (f32[128,4]{0,1:T(4,128)S(1)}, f32[128,4]{0,1:T(4,128)}, u32[]{:S(2)}) copy-start(f32[128,4]{0,1:T(4,128)} %param.53) | copy-start | bytes 6148
  255.1 6.5 %copy-start.1 = (bf16[128,2048]{1,0:T(8,128)(2,1)S(1)}, bf16[128,2048]{1,0:T(8,128)(2,1)}, u32[]{:S(2)}) copy-start(bf16[128,2048]{1,0:T(8,128)(2,1)} %get-tuple-element.9) | copy-start | bytes 1572868
  255.1 47.1 %all-to-all-start.1 = ((bf16[128,24,512]{2,1,0:T(8,128)(2,1)}), bf16[128,24,512]{2,1,0:T(8,128)(2,1)}, u32[]{:S(2)}, u32[]{:S(2)}) async-start(bf16[128,24,512]{2,1,0:T(8,128)(2,1)} %bitcast.30), calls=%async_computation.1 | async-start | bytes 6291456 | tf_op jit(solution)/shard_map/all_to_all | solution.py:451

commit v2 on v1

v2 whole, which is shorter than its diff:
```python
import functools

import jax
import jax.numpy as jnp
import numpy as np
from jax import lax
from jax.experimental import pallas as pl
from jax.experimental.pallas import tpu as pltpu
from jax.sharding import PartitionSpec as P

D = 2048
TOPK = 4
EPS = 1e-06
TQ = 128
LOG2E = 1.4426950408889634
RC = 256
CAP = 6
PIECES = 4
WIDTH = D // PIECES
SLAB = PIECES * CAP
EXPERTS = 128
GROUP = 16
GROUP_ROWS = GROUP * SLAB
ATTN_BYTES = 60 * 2**20
VMEM_BYTES = 60 * 2**20
MESH = pl.DeviceIdType.MESH
ORDERS = ((0, 1, 2), (1, 2, 0), (2, 0, 1))
STRIDE = (1, 4, 16)

CHUNKS = ((0, 64), (64, 64), (128, 64), (192, 32), (224, 32))
SPANS = (5, 5, 5, 3, 3)
STARTS = (0, 5, 10, 15, 18)
STEPS = 21
TURNS = {1: 2, 2: 7, 3: 11, 4: 14}
KEYS = 1024


def attn_kernel(
    qn_in, qw_in, kn_in, vn_in, kw_in, vw_in, lamn, lamw, gn, gw, relpos,
    kvall, out,
    kv, buf, qgot_n, qgot_w, qn, qw, mn, mw, accn, accw, lw, att, fin,
    isem, osem, qs, qr, ssem, rsem, bsem, ds, dr,
):
    sp = lax.axis_index("sp")
    tp = lax.axis_index("tp")
    half = sp // 32
    at = (sp % 4, (sp // 4) % 4, sp // 16)
    mirror = 63 - sp

    def dev(d, by):
        return (sp + ((at[d] + by) % 4 - at[d]) * STRIDE[d], tp)

    loads = []
    for i, (src, lo, n) in enumerate(
        ((kn_in, 0, 128), (vn_in, 128, 128), (kw_in, 256, 256), (vw_in, 512, 256))
    ):
        copy = pltpu.make_async_copy(src, kv.at[:, pl.ds(lo, n)], isem.at[i])
        copy.start()
        loads.append(copy)

    barrier = pltpu.get_barrier_semaphore()
    for d in range(3):
        for by in (1, 3):
            pl.semaphore_signal(barrier, inc=1, device_id=dev(d, by), device_id_type=MESH)
    for who in ((sp, 1 - tp), (mirror, tp), (mirror, 1 - tp)):
        pl.semaphore_signal(barrier, inc=1, device_id=who, device_id_type=MESH)
    pl.semaphore_wait(barrier, 9)
    for copy in loads:
        copy.wait()
    own = pltpu.make_async_copy(kv, kvall.at[at[2], at[1], at[0]], osem)
    own.start()

    def region(c, p, shift, lo, n):
        order = ORDERS[c]
        idx = [at[0], at[1], at[2]]
        for d in order[:p]:
            idx[d] = slice(None)
        idx[order[p]] = (at[order[p]] + shift) % 4
        return kvall.at[idx[2], idx[1], idx[0], pl.ds(lo, n), pl.ds(256 * c, 256)]

    def send(c, p, k, src, dst, by, chunk=0):
        s = (c * 7 + p + chunk) * 6 + k
        return pltpu.make_async_remote_copy(
            src_ref=src, dst_ref=dst, send_sem=ssem.at[s], recv_sem=rsem.at[s],
            device_id=dev(ORDERS[c][p], by), device_id_type=MESH,
        )

    def direct(c, p, lo, n, chunk, later):
        m = n // 2
        found = []
        for k, by in ((0, 1), (1, 3)):
            at_row = lo + m * ((k + later) % 2)
            dst = region(c, p, 0, at_row, m)
            src = kv.at[pl.ds(at_row, m), pl.ds(256 * c, 256)] if p == 0 else dst
            found.append(send(c, p, k + 2 * later, src, dst, by, chunk))
        return found

    def passed(c, p, lo, n, chunk):
        m = n // 2
        r1 = region(c, p, 3, lo, m)
        r2 = region(c, p, 1, lo + m, m)
        return send(c, p, 4, r1, r1, 1, chunk), send(c, p, 5, r2, r2, 3, chunk)

    def begin(p, lo=0, n=256, chunk=0):
        for later in range(2):
            for c in range(3):
                for x in direct(c, p, lo, n, chunk, later):
                    x.start()

    def middle(p, lo=0, n=256, chunk=0):
        for c in range(3):
            for x, y in zip(direct(c, p, lo, n, chunk, 0), passed(c, p, lo, n, chunk)):
                x.wait_recv()
                y.start()

    def end(p, lo=0, n=256, chunk=0):
        for c in range(3):
            for x in (*direct(c, p, lo, n, chunk, 1), *passed(c, p, lo, n, chunk)):
                x.wait_recv()

    def drain(p, lo=0, n=256, chunk=0):
        for c in range(3):
            for later in range(2):
                for x in direct(c, p, lo, n, chunk, later):
                    x.wait_send()
            for x in passed(c, p, lo, n, chunk):
                x.wait_send()

    def queries(k, src, dst):
        return pltpu.make_async_remote_copy(
            src_ref=src.at[pl.ds((1 - half) * TQ, TQ), :], dst_ref=dst, send_sem=qs.at[k],
            recv_sem=qr.at[k], device_id=(mirror, tp), device_id_type=MESH,
        )

    qcopies = (queries(0, qn_in, qgot_n), queries(1, qw_in, qgot_w))
    begin(0)
    middle(0)
    own.wait()
    end(0)
    begin(1)
    for x in qcopies:
        x.start()
    middle(1)
    end(1)
    begin(2, *CHUNKS[0], 0)

    for x in qcopies:
        x.wait_recv()
    lane = lax.broadcasted_iota(jnp.int32, (TQ, 128), 1)
    zero = jnp.zeros((TQ, 128), jnp.bfloat16)
    for mine in (1, 0):
        tile = 1 - half if mine else half
        for h in range(4):
            col = slice(h * 128, (h + 1) * 128)
            rows = qn_in[pl.ds(half * TQ, TQ), col] if mine else qgot_n[:, col]
            qn[tile, h * TQ : (h + 1) * TQ, :] = jnp.where(lane < 64, rows, zero)
            qn[tile, (4 + h) * TQ : (5 + h) * TQ, :] = jnp.where(lane < 64, zero, rows)
        for h in range(2):
            for m in range(2):
                col = slice(h * 256 + m * 128, h * 256 + (m + 1) * 128)
                rows = qw_in[pl.ds(half * TQ, TQ), col] if mine else qgot_w[:, col]
                put = slice((2 * m + h) * TQ, (2 * m + h + 1) * TQ)
                qw[tile, put, m * 128 : (m + 1) * 128] = rows
                qw[tile, put, (1 - m) * 128 : (2 - m) * 128] = zero
    mn[...] = jnp.full(mn.shape, -1e30, jnp.float32)
    mw[...] = jnp.full(mw.shape, -1e30, jnp.float32)
    accn[...] = jnp.zeros(accn.shape, jnp.float32)
    accw[...] = jnp.zeros(accw.shape, jnp.float32)
    lw[...] = jnp.zeros(lw.shape, jnp.float32)

    middle(2, *CHUNKS[0], 0)
    begin(2, *CHUNKS[1], 1)

    low = half * mirror + (1 - half) * sp
    high = 63 - low

    def place(s):
        after = [(s >= start).astype(jnp.int32) for start in STARTS]
        j = s - sum(SPANS[k - 1] * after[k] for k in range(1, len(CHUNKS)))
        width = 16 + 16 * after[3]
        n_hi = high // width + 1
        n_lo = low // width + 1
        turned = half * after[4]
        first = n_hi * (1 - turned) + n_lo * turned
        second = (j >= first).astype(jnp.int32)
        tile = turned + second - 2 * turned * second
        g = j - second * first
        last = n_hi * (1 - tile) + n_lo * tile - 1
        row = sum((CHUNKS[k][0] - CHUNKS[k - 1][0]) * after[k] for k in range(1, len(CHUNKS)))
        return after, row, tile, g, g == last, g * width * 256 + row

    def fetch(s, slot):
        after, row, _, g, _, _ = place(s)

        @pl.when(after[3] == 0)
        def _():
            for k in range(16):
                pltpu.make_async_copy(
                    kvall.at[g, k // 4, k % 4, pl.ds(pl.multiple_of(row, 32), 64), :],
                    buf.at[slot, k // 4, pl.ds((k % 4) * 64, 64), :], bsem.at[slot],
                ).start()

        @pl.when(after[3] == 1)
        def _():
            for k in range(32):
                pltpu.make_async_copy(
                    kvall.at[2 * g + k // 16, k // 4 % 4, k % 4, pl.ds(pl.multiple_of(row, 32), 32), :],
                    buf.at[slot, k // 8, pl.ds((k % 8) * 32, 32), :], bsem.at[slot],
                ).start()

    def finish(tile):
        for h in range(4):
            r0, r1 = h * TQ, (4 + h) * TQ
            d = accn[tile, r0 : r0 + TQ, 0:128] / accn[tile, r0 : r0 + TQ, 128:256] - lamn[h] * (
                accn[tile, r1 : r1 + TQ, 0:128] / accn[tile, r1 : r1 + TQ, 128:256]
            )
            d = d * lax.rsqrt(jnp.mean(d * d, axis=-1, keepdims=True) + EPS) * gn[...]
            att[tile, :, h * 128 : (h + 1) * 128] = d.astype(jnp.bfloat16)
        for h in range(2):
            r0, r1 = h * TQ, (2 + h) * TQ
            l0 = jnp.sum(lw[tile, r0 : r0 + TQ, :], axis=-1, keepdims=True)
            l1 = jnp.sum(lw[tile, r1 : r1 + TQ, :], axis=-1, keepdims=True)
            d = accw[tile, r0 : r0 + TQ, :] / l0 - lamw[h] * (accw[tile, r1 : r1 + TQ, :] / l1)
            d = d * lax.rsqrt(jnp.mean(d * d, axis=-1, keepdims=True) + EPS) * gw[...]
            att[tile, :, 512 + h * 256 : 512 + (h + 1) * 256] = d.astype(jnp.bfloat16)

    def deliver(k, tile, who):
        return pltpu.make_async_remote_copy(
            src_ref=att.at[tile], dst_ref=fin.at[tp], send_sem=ds.at[k], recv_sem=dr.at[tp],
            device_id=who, device_id_type=MESH,
        )

    def step(s, carry):
        slot = s % 2
        after, _, tile, g, masked, first_key = place(s)
        for chunk in range(len(CHUNKS)):
            @pl.when(s == STARTS[chunk])
            def _():
                end(2, *CHUNKS[chunk], chunk)
                fetch(s, slot)
        for chunk, turn in TURNS.items():
            @pl.when(s == turn)
            def _():
                middle(2, *CHUNKS[chunk], chunk)
                if chunk + 1 < len(CHUNKS):
                    begin(2, *CHUNKS[chunk + 1], chunk + 1)

        @pl.when(s == STEPS - 1 - half)
        def _():
            finish(half)
            deliver(0, half, (mirror, half)).start()

        pltpu.make_async_copy(kvall.at[0, 0], buf.at[slot], bsem.at[slot]).wait()

        more = s + 1 < STEPS
        for start in STARTS[1:]:
            more = more & (s + 1 != start)

        @pl.when(more)
        def _():
            fetch(s + 1, 1 - slot)

        base = half * TQ + (high * (1 - tile) + low * tile) * 256

        def attend(mask):
            def columns(lo, n):
                return buf[slot, :, :, lo : lo + n].reshape(KEYS, n)

            keys_n, keys_w, vals_w = columns(0, 128), columns(256, 256), columns(512, 256)
            vals_n = jnp.concatenate(
                [columns(128, 128), jnp.ones((KEYS, 128), jnp.bfloat16)], axis=1
            )
            dims = (((1,), (1,)), ((), ()))
            if mask:
                row = lax.broadcasted_iota(jnp.int32, (RC, KEYS), 0) % TQ
                keep = (relpos[after[3]] + first_key) <= (row + base)

            def scores(narrow, r):
                if narrow:
                    return lax.dot_general(
                        qn[tile, r : r + RC, :], keys_n, dims, preferred_element_type=jnp.float32
                    )
                return lax.dot_general(
                    qw[tile, r : r + RC, :], keys_w, dims, preferred_element_type=jnp.float32
                )

            parts = [(True, r) for r in range(0, 8 * TQ, RC)]
            parts += [(False, r) for r in range(0, 4 * TQ, RC)]
            following = scores(*parts[0])
            for i, (narrow, r) in enumerate(parts):
                sc = following
                if i + 1 < len(parts):
                    following = scores(*parts[i + 1])
                m_ref = mn if narrow else mw
                sc = sc * ((64 if narrow else 128) ** -0.5 * LOG2E)
                if mask:
                    sc = jnp.where(keep, sc, -1e30)
                m_old = m_ref[tile, r : r + RC, :]
                m_new = jnp.maximum(m_old, jnp.max(sc, axis=-1, keepdims=True))
                m_ref[tile, r : r + RC, :] = m_new
                alpha = jnp.exp2(m_old - m_new)
                p = jnp.exp2(sc - jnp.tile(m_new, (1, KEYS // 128)))
                pb = p.astype(jnp.bfloat16)
                twice = jnp.tile(alpha, (1, 2))
                if narrow:
                    accn[tile, r : r + RC, :] = accn[tile, r : r + RC, :] * twice + jnp.dot(
                        pb, vals_n, preferred_element_type=jnp.float32
                    )
                else:
                    ps = p[:, 0:128]
                    for j in range(1, KEYS // 128):
                        ps = ps + p[:, j * 128 : (j + 1) * 128]
                    lw[tile, r : r + RC, :] = lw[tile, r : r + RC, :] * alpha + ps
                    accw[tile, r : r + RC, :] = accw[tile, r : r + RC, :] * twice + jnp.dot(
                        pb, vals_w, preferred_element_type=jnp.float32
                    )

        @pl.when(jnp.logical_not(masked))
        def _():
            attend(False)

        @pl.when(masked)
        def _():
            attend(True)

        return carry

    lax.fori_loop(0, STEPS, step, 0)

    finish(1 - half)

    @pl.when(tp != half)
    def _():
        deliver(1, 1 - half, (sp, 1 - tp)).start()

    drain(0)
    drain(1)
    for chunk in range(len(CHUNKS)):
        drain(2, *CHUNKS[chunk], chunk)
    for x in qcopies:
        x.wait_send()

    def arrived(slot):
        pltpu.make_async_remote_copy(
            src_ref=att.at[0], dst_ref=fin.at[slot], send_sem=ds.at[0], recv_sem=dr.at[slot],
            device_id=(mirror, half), device_id_type=MESH,
        ).wait_recv()

    @pl.when(tp == half)
    def _():
        arrived(1 - tp)
        out[pl.ds(tp, 1)] = att[pl.ds(1 - half, 1)]
        out[pl.ds(1 - tp, 1)] = fin[pl.ds(1 - tp, 1)]

    @pl.when(tp != half)
    def _():
        arrived(0)
        arrived(1)
        out[...] = fin[...]
        deliver(1, 1 - half, (sp, 1 - tp)).wait_send()

    deliver(0, half, (mirror, half)).wait_send()


def attention(qn, qw, kn, vn, kw, vw, lamn, lamw, gn, gw):
    col = np.arange(KEYS)
    rel = np.stack([(col // n) * 256 + col % n for n in (64, 32)]).astype(np.int32)
    vmem = pl.BlockSpec(memory_space=pltpu.VMEM)
    smem = pl.BlockSpec(memory_space=pltpu.SMEM)
    hbm = pl.BlockSpec(memory_space=pltpu.HBM)
    f32, bf16 = jnp.float32, jnp.bfloat16
    dma = pltpu.SemaphoreType.DMA
    _, out = pl.pallas_call(
        attn_kernel,
        in_specs=[vmem, vmem, hbm, hbm, hbm, hbm, smem, smem, vmem, vmem, vmem],
        out_specs=(hbm, vmem),
        out_shape=(
            jax.ShapeDtypeStruct((4, 4, 4, 256, 768), bf16),
            jax.ShapeDtypeStruct((2, TQ, 1024), bf16),
        ),
        scratch_shapes=[
            pltpu.VMEM((256, 768), bf16),
            pltpu.VMEM((2, 4, 256, 768), bf16),
            pltpu.VMEM((TQ, 512), bf16),
            pltpu.VMEM((TQ, 512), bf16),
            pltpu.VMEM((2, 8 * TQ, 128), bf16),
            pltpu.VMEM((2, 4 * TQ, 256), bf16),
            pltpu.VMEM((2, 8 * TQ, 128), f32),
            pltpu.VMEM((2, 4 * TQ, 128), f32),
            pltpu.VMEM((2, 8 * TQ, 256), f32),
            pltpu.VMEM((2, 4 * TQ, 256), f32),
            pltpu.VMEM((2, 4 * TQ, 128), f32),
            pltpu.VMEM((2, TQ, 1024), bf16),
            pltpu.VMEM((2, TQ, 1024), bf16),
            dma((4,)),
            dma,
            dma((2,)),
            dma((2,)),
            dma((126,)),
            dma((126,)),
            dma((2,)),
            dma((2,)),
            dma((2,)),
        ],
        compiler_params=pltpu.CompilerParams(
            collective_id=3, has_side_effects=True, vmem_limit_bytes=ATTN_BYTES
        ),
        cost_estimate=pl.CostEstimate(
            flops=30 * 10**9, bytes_accessed=60 * 10**6, transcendentals=0
        ),
        name="attention",
    )(
        qn, qw, kn, vn, kw, vw, lamn, lamw, gn.reshape(1, 128), gw.reshape(1, 256),
        jnp.asarray(rel.reshape(2, 1, KEYS)),
    )
    return out


def rms(v, gain):
    return v * lax.rsqrt(jnp.mean(v * v, axis=-1, keepdims=True) + EPS) * gain


def dot(a, b):
    return jnp.dot(a, b, preferred_element_type=jnp.float32)


def ranks(ids):
    lane = lax.broadcasted_iota(jnp.int32, (TQ, EXPERTS), 1)
    named = jnp.zeros((TQ, EXPERTS), jnp.float32)
    for k in range(TOPK):
        named = named + (ids[:, k : k + 1] == lane).astype(jnp.float32)
    below = lax.broadcasted_iota(jnp.int32, (TQ, TQ), 1) < lax.broadcasted_iota(
        jnp.int32, (TQ, TQ), 0
    )
    count = dot(below.astype(jnp.bfloat16), named.astype(jnp.bfloat16))
    return (named * (count + 1.0)).astype(jnp.bfloat16)


def mid_kernel(
    f, on, ow, stream, gmix, gffn, ids, rank_of, piece_mask, mixed_out, normed_out, slab
):
    projected = (
        dot(f[0, :, 0:512], on[0:512, :])
        + dot(f[1, :, 0:512], on[512:1024, :])
        + dot(f[0, :, 512:1024], ow[0:512, :])
        + dot(f[1, :, 512:1024], ow[512:1024, :])
    )
    mixed = (stream[...].astype(jnp.float32) + rms(projected, gmix[...])).astype(jnp.bfloat16)
    mixed_out[...] = mixed
    normed = rms(mixed.astype(jnp.float32), gffn[...]).astype(jnp.bfloat16)
    normed_out[...] = normed
    stacked = jnp.concatenate([normed[:, c * WIDTH : (c + 1) * WIDTH] for c in range(PIECES)], 0)
    value = ranks(ids[...])
    row = lax.broadcasted_iota(jnp.int32, (GROUP_ROWS, EXPERTS), 0)
    lane = lax.broadcasted_iota(jnp.int32, (GROUP_ROWS, EXPERTS), 1)
    for g in range(EXPERTS // GROUP):
        low = (lane - g * GROUP) * SLAB
        spread = ((row >= low) & (row < low + SLAB)).astype(jnp.bfloat16)
        here = lax.dot_general(
            spread, value, (((1,), (1,)), ((), ())), preferred_element_type=jnp.float32
        )
        chosen = (here == rank_of[...]).astype(jnp.float32).astype(jnp.bfloat16)
        chosen = jnp.concatenate([chosen] * PIECES, axis=1) * piece_mask[...]
        slab[g * GROUP_ROWS : (g + 1) * GROUP_ROWS, :] = dot(chosen, stacked).astype(jnp.bfloat16)


def slab_tables():
    i = np.arange(GROUP_ROWS) % SLAB
    rank = np.broadcast_to((i % CAP + 1)[:, None], (GROUP_ROWS, EXPERTS)).astype(np.float32)
    piece = (i // CAP)[:, None] == (np.arange(PIECES * TQ) // TQ)[None, :]
    return rank, piece.astype(np.float32)


def order_table():
    i = np.arange(GROUP_ROWS)
    to = (i % SLAB // CAP) * (GROUP * CAP) + (i // SLAB) * CAP + i % CAP
    table = np.zeros((GROUP_ROWS, GROUP_ROWS), np.float32)
    table[to, i] = 1.0
    return table


def mid(f, on, ow, stream, gmix, gffn, ids):
    rank, piece = slab_tables()
    return pl.pallas_call(
        mid_kernel,
        out_shape=(
            jax.ShapeDtypeStruct((TQ, D), jnp.bfloat16),
            jax.ShapeDtypeStruct((TQ, D), jnp.bfloat16),
            jax.ShapeDtypeStruct((EXPERTS * SLAB, WIDTH), jnp.bfloat16),
        ),
        compiler_params=pltpu.CompilerParams(vmem_limit_bytes=VMEM_BYTES),
        cost_estimate=pl.CostEstimate(flops=4 * 10**9, bytes_accessed=14 * 10**6, transcendentals=0),
        name="mid",
    )(
        f,
        on,
        ow,
        stream,
        gmix.reshape(1, D),
        gffn.reshape(1, D),
        ids,
        jnp.asarray(rank),
        jnp.asarray(piece, jnp.bfloat16),
    )


def expert_kernel(x, g1, u1, d1, g2, u2, d2, order, order_t, out, rows, results):
    span = GROUP * CAP
    for g in range(EXPERTS // GROUP):
        got = dot(order[...], x[g * GROUP_ROWS : (g + 1) * GROUP_ROWS, :]).astype(jnp.bfloat16)
        for c in range(PIECES):
            rows[g * span : (g + 1) * span, c * WIDTH : (c + 1) * WIDTH] = got[
                c * span : (c + 1) * span, :
            ]
    for m in range(0, EXPERTS * CAP, 256):
        part = rows[m : m + 256, :]
        total = None
        for gate, up, down in ((g1, u1, d1), (g2, u2, d2)):
            gated = dot(part, gate[0])
            hidden = (gated / (1.0 + jnp.exp(-gated)) * dot(part, up[0])).astype(jnp.bfloat16)
            term = dot(hidden, down[0])
            total = term if total is None else total + term
        results[m : m + 256, :] = total.astype(jnp.bfloat16)
    for g in range(EXPERTS // GROUP):
        stacked = jnp.concatenate(
            [
                results[g * span : (g + 1) * span, c * WIDTH : (c + 1) * WIDTH]
                for c in range(PIECES)
            ],
            0,
        )
        out[g * GROUP_ROWS : (g + 1) * GROUP_ROWS, :] = dot(order_t[...], stacked).astype(
            jnp.bfloat16
        )


def run_expert(which, x, gate, up, down, gate2, up2, down2):
    table = order_table()
    full = lambda *shape: pl.BlockSpec(shape, lambda i, w: (0,) * len(shape))
    mine = lambda *shape: pl.BlockSpec((1, *shape), lambda i, w: (w[0], 0, 0))
    half = gate.shape[2]
    return pl.pallas_call(
        expert_kernel_with_prefetch,
        grid_spec=pltpu.PrefetchScalarGridSpec(
            num_scalar_prefetch=1,
            grid=(1,),
            in_specs=[
                full(EXPERTS * SLAB, WIDTH),
                mine(D, half),
                mine(D, half),
                mine(half, D),
                full(1, D, half),
                full(1, D, half),
                full(1, half, D),
                full(GROUP_ROWS, GROUP_ROWS),
                full(GROUP_ROWS, GROUP_ROWS),
            ],
            out_specs=full(EXPERTS * SLAB, WIDTH),
            scratch_shapes=[
                pltpu.VMEM((EXPERTS * CAP, D), jnp.bfloat16),
                pltpu.VMEM((EXPERTS * CAP, D), jnp.bfloat16),
            ],
        ),
        out_shape=jax.ShapeDtypeStruct((EXPERTS * SLAB, WIDTH), jnp.bfloat16),
        compiler_params=pltpu.CompilerParams(vmem_limit_bytes=VMEM_BYTES),
        cost_estimate=pl.CostEstimate(flops=6 * 10**9, bytes_accessed=14 * 10**6, transcendentals=0),
        name="expert",
    )(
        which,
        x,
        gate,
        up,
        down,
        gate2,
        up2,
        down2,
        jnp.asarray(table, jnp.bfloat16),
        jnp.asarray(table.T, jnp.bfloat16),
    )


def expert_kernel_with_prefetch(which, *refs):
    expert_kernel(*refs)


def combine_kernel(back, ids, weights, shared, mixed, gpost, rank_row, piece_row, out):
    value = ranks(ids[...])
    lane = lax.broadcasted_iota(jnp.int32, (TQ, EXPERTS), 1)
    share = jnp.zeros((TQ, EXPERTS), jnp.float32)
    for k in range(TOPK):
        share = share + jnp.where(ids[:, k : k + 1] == lane, weights[:, k : k + 1], 0.0)
    share = share.astype(jnp.bfloat16)
    row = lax.broadcasted_iota(jnp.int32, (EXPERTS, GROUP_ROWS), 0)
    col = lax.broadcasted_iota(jnp.int32, (EXPERTS, GROUP_ROWS), 1)
    total = jnp.zeros((PIECES * TQ, WIDTH), jnp.float32)
    for g in range(EXPERTS // GROUP):
        low = (row - g * GROUP) * SLAB
        spread = ((col >= low) & (col < low + SLAB)).astype(jnp.bfloat16)
        held = jnp.where(dot(value, spread) == rank_row[...], dot(share, spread), 0.0)
        picks = jnp.concatenate(
            [jnp.where(piece_row[...] == float(c), held, 0.0) for c in range(PIECES)], 0
        ).astype(jnp.bfloat16)
        total = total + dot(picks, back[g * GROUP_ROWS : (g + 1) * GROUP_ROWS, :])
    routed = jnp.concatenate([total[c * TQ : (c + 1) * TQ, :] for c in range(PIECES)], axis=1)
    combined = shared[...] + routed
    out[...] = (mixed[...].astype(jnp.float32) + rms(combined, gpost[...])).astype(jnp.bfloat16)


def combine(back, ids, weights, shared, mixed, gpost):
    i = np.arange(GROUP_ROWS) % SLAB
    return pl.pallas_call(
        combine_kernel,
        out_shape=jax.ShapeDtypeStruct((TQ, D), jnp.bfloat16),
        compiler_params=pltpu.CompilerParams(vmem_limit_bytes=VMEM_BYTES),
        cost_estimate=pl.CostEstimate(flops=3 * 10**9, bytes_accessed=6 * 10**6, transcendentals=0),
        name="combine",
    )(
        back,
        ids,
        weights,
        shared,
        mixed,
        gpost.reshape(1, D),
        jnp.asarray((i % CAP + 1)[None, :], jnp.float32),
        jnp.asarray((i // CAP)[None, :], jnp.float32),
    )


BOTH = ("sp", "tp")


def exchanged(slab):
    pieces = slab.reshape(EXPERTS, SLAB, WIDTH)
    return lax.all_to_all(pieces, BOTH, 0, 0, tiled=True).reshape(EXPERTS * SLAB, WIDTH)


def shards(
    queries_narrow,
    keys_narrow,
    values_narrow,
    queries_wide,
    keys_wide,
    values_wide,
    lambda_narrow,
    lambda_wide,
    gain_narrow,
    gain_wide,
    out_narrow,
    out_wide,
    stream,
    gain_mix,
    gain_ffn,
    gain_post,
    shared_gate,
    shared_up,
    shared_down,
    expert_gate,
    expert_up,
    expert_down,
    expert_ids,
    route_weights,
):
    tp = lax.axis_index("tp")
    across = [(0, 1), (1, 0)]
    other = [
        lax.ppermute(lax.dynamic_slice_in_dim(w, 1 - tp, 1, 0), "tp", across)
        for w in (expert_gate, expert_up, expert_down)
    ]
    attended = attention(
        queries_narrow,
        queries_wide,
        keys_narrow,
        values_narrow,
        keys_wide,
        values_wide,
        lambda_narrow,
        lambda_wide,
        gain_narrow,
        gain_wide,
    )
    mixed, normed, slab = mid(
        attended, out_narrow, out_wide, stream, gain_mix, gain_ffn, expert_ids
    )
    incoming = exchanged(slab)
    results = run_expert(
        jnp.reshape(tp, (1,)).astype(jnp.int32),
        incoming,
        expert_gate,
        expert_up,
        expert_down,
        *other,
    )
    back = exchanged(results)
    shared_hidden = (
        jax.nn.silu(dot(normed, shared_gate)) * dot(normed, shared_up)
    ).astype(jnp.bfloat16)
    shared_out = dot(shared_hidden, shared_down)
    return combine(back, expert_ids, route_weights, shared_out, mixed, gain_post)


def solution(mesh):
    return jax.shard_map(
        shards,
        mesh=mesh,
        in_specs=(
            P("sp", "tp"),
            P("sp", "tp"),
            P("sp", "tp"),
            P("sp", "tp"),
            P("sp", "tp"),
            P("sp", "tp"),
            P("tp"),
            P("tp"),
            P(),
            P(),
            P(),
            P(),
            P(("sp", "tp"), None),
            P(),
            P(),
            P(),
            P(),
            P(),
            P(),
            P("sp", None, "tp"),
            P("sp", None, "tp"),
            P("sp", "tp", None),
            P(("sp", "tp"), None),
            P(("sp", "tp"), None),
        ),
        out_specs=P(("sp", "tp"), None),
        check_vma=False,
    )
```

time: 310 us -> 266 us (0.86)
  starting transfers between devices: 32.6 us -> 16.3 us
  Pallas kernels: 178 us -> 167 us
  waiting for transfers between devices: 81.8 us -> 71.4 us
  other arithmetic: 5.31 us -> 0 us
    ppermute x3 -> x0, starting transfers between devices: 20.5 us -> none  [the longest x1 9.32 us: shards(): a = lax.ppermute(jnp.where(tp == 0, own, away), BOTH, first)]
    pallas_call x2 -> x1, Pallas kernels: 146 us -> 136 us  [attention(): pl.pallas_call(attn_kernel, in_specs=[vmem, vmem, hbm, hbm, hbm, hbm, sme...]
    ppermute x3 -> x0, waiting for transfers between devices: 10.4 us -> none  [the longest x1 9.52 us: shards(): b = lax.ppermute(jnp.where(tp == 0, away, own), BOTH, second)]
    all_to_all x2, starting transfers between devices: 10.4 us -> 14.1 us  [exchanged(): lax.all_to_all(pieces, BOTH, 0, 0, tiled=True)]
  transfers between devices with their start and end apart: 8 -> 5, of which waited for: 7 -> 5; matrix products, arithmetic and copies ran while one was open for 4% -> 3% of each run, Pallas kernels for 33% -> 0%
where the time goes in v2:
time: 266 us; the launch traced here: 265 us
  Pallas kernels  167 us (63%)
  waiting for transfers between devices  71.4 us (27%)
  starting transfers between devices  16.3 us (6%)
  matrix products  5.46 us (2%)
  local copies, waits for them, and re-layouts  4.94 us (2%)
    pallas_call x1, Pallas kernels, attention(): pl.pallas_call(attn_kernel, in_specs=[vmem, vmem, hbm, hbm, hbm, hbm, sme...  136 us
    all_to_all x2, waiting for transfers between devices, exchanged(): lax.all_to_all(pieces, BOTH, 0, 0, tiled=True)  68.2 us
    all_to_all x2, starting transfers between devices, exchanged(): lax.all_to_all(pieces, BOTH, 0, 0, tiled=True)  14.1 us
    pallas_call x1, Pallas kernels, run_expert(): pl.pallas_call(expert_kernel_with_prefetch, grid_spec=pltpu.PrefetchScala...  14.1 us
    pallas_call x1, Pallas kernels, mid(): pl.pallas_call(mid_kernel, out_shape=(jax.ShapeDtypeStruct((TQ, D), jnp.b...  10 us
    pallas_call x1, Pallas kernels, combine(): pl.pallas_call(combine_kernel, out_shape=jax.ShapeDtypeStruct((TQ, D), jn...  7.18 us
    dot_general x2, matrix products, dot(): return jnp.dot(a, b, preferred_element_type=jnp.float32)  5.46 us
  transfers between devices with their start and end apart: 5, of which 5 were waited for; matrix products, arithmetic and copies ran while one was open for 3% of the time, Pallas kernels for 0%

profile of v2, /device:TPU:1, one launch (start us, length us, event | category | flops | bytes accessed | tf_op | source)
XLA Modules:
  0.0 265.4 jit_solution(2674735883953167982)
XLA Ops:
  0.0 1.6 copy.32.ids
  1.6 135.8 %attention.1 = (bf16[4,4,4,256,768]{4,3,2,1,0:T(8,128)(2,1)}, bf16[2,128,1024]{2,1,0:T(8,128)(2,1)}) custom-call(bf16[256,512]{1,0:T(8,128)(2,1)} %qn_in.1, bf16[256,512]{1,0:T(8,128)(2,1)} %qw_in.1, bf16[256,128]{1,0:T(8,128)(2,1)} %kn_in.1, bf16[256,128]{1,0:T(8,128)(2,1)} %vn_in.1, bf16[256,256]{1,0:T(8,128)(2,1)} %kw_in.1, bf16[256,256]{1,0:T(8,128)(2,1)} %vw_in.1, ...), custom_call_target="tpu_custom_call" | custom-call | flops 30000001024 | bytes 60000000 | tf_op jit(solution)/shard_map/attention/pallas_call | solution.py:373
  137.4 10.0 %mid.1 = (bf16[128,2048]{1,0:T(8,128)(2,1)}, bf16[128,2048]{1,0:T(8,128)(2,1)}, bf16[3072,512]{1,0:T(8,128)(2,1)}) custom-call(bf16[2,128,1024]{2,1,0:T(8,128)(2,1)} %get-tuple-element.9.f, bf16[1024,2048]{1,0:T(8,128)(2,1)} %on.1, bf16[1024,2048]{1,0:T(8,128)(2,1)} %ow.1, bf16[128,2048]{1,0:T(8,128)(2,1)} %stream.1, f32[1,2048]{1,0:T(1,128)} %bitcast.17, ...), custom_call_target="tpu_custom_call" | custom-call | flops 4000000000 | bytes 14000000 | tf_op jit(solution)/shard_map/mid/pallas_call | solution.py:484
  147.4 8.4 %all-to-all-start = ((bf16[128,24,512]{2,1,0:T(8,128)(2,1)}), bf16[128,24,512]{2,1,0:T(8,128)(2,1)}, u32[]{:S(2)}, u32[]{:S(2)}) async-start(bf16[128,24,512]{2,1,0:T(8,128)(2,1)} %bitcast.15), calls=%async_computation | async-start | bytes 6291456 | tf_op jit(solution)/shard_map/all_to_all | solution.py:634
  155.8 0.0 copy-start.2
  155.8 0.0 copy-start.3
  155.8 1.4 constant_dynamic-slice_fusion.2
  157.2 1.2 collective-permute-start
  158.5 0.1 constant_dynamic-slice_fusion.1
  158.5 0.4 collective-permute-start.1
  159.0 0.1 constant_dynamic-slice_fusion
  159.1 0.6 collective-permute-start.2
  159.6 1.1 collective-permute-done.refs_4_
  160.7 1.5 collective-permute-done.1.refs_5_
  162.2 1.0 copy-done.6
  163.3 0.6 collective-permute-done.2.refs_6_
  163.9 33.1 %all-to-all-done = bf16[128,24,512]{2,1,0:T(8,128)(2,1)} async-done(((bf16[128,24,512]{2,1,0:T(8,128)(2,1)}), bf16[128,24,512]{2,1,0:T(8,128)(2,1)}, u32[]{:S(2)}, u32[]{:S(2)}) %all-to-all-start) | async-done | bytes 3145760 | tf_op jit(solution)/shard_map/all_to_all | solution.py:634
  196.9 14.1 %expert.1 = bf16[3072,512]{1,0:T(8,128)(2,1)} custom-call(s32[1]{0:T(128)} %bitcast.which, bf16[3072,512]{1,0:T(8,128)(2,1)} %bitcast.6.refs_0_, bf16[2,2048,256]{2,1,0:T(8,128)(2,1)} %refs_1_.1, bf16[2,2048,256]{2,1,0:T(8,128)(2,1)} %refs_2_.1, bf16[2,256,2048]{2,1,0:T(8,128)(2,1)} %refs_3_.1, bf16[1,2048,256]{2,1,0:T(8,128)(2,1)} %copy-done.5, ...), custom_call_target="tpu_custom_call" | custom-call | flops 6000000000 | bytes 14000000 | tf_op jit(solution)/shard_map/expert/pallas_call | solution.py:542
  211.1 5.8 %all-to-all-start.1 = ((bf16[128,24,512]{2,1,0:T(8,128)(2,1)}), bf16[128,24,512]{2,1,0:T(8,128)(2,1)}, u32[]{:S(2)}, u32[]{:S(2)}) async-start(bf16[128,24,512]{2,1,0:T(8,128)(2,1)} %bitcast.16), calls=%async_computation.1 | async-start | bytes 6291456 | tf_op jit(solution)/shard_map/all_to_all | solution.py:634
  216.9 0.7 copy.34.weights
  217.6 2.0 fusion.9
  219.7 3.4 %fusion.1.shared = f32[128,2048]{1,0:T(8,128)} fusion(bf16[512,2048]{1,0:T(8,128)(2,1)S(1)} %copy-done, bf16[128,2048]{1,0:T(8,128)(2,1)S(1)} %copy-done.1, bf16[2048,512]{1,0:T(8,128)(2,1)} %param.48, f32[128,512]{1,0:T(8,128)S(1)} %fusion.9), kind=kOutput, calls=%fused_computation.2 | convolution fusion | flops 537264128 | bytes 6029312 | tf_op jit(solution)/shard_map/dot_general | solution.py:424
  223.1 35.1 %all-to-all-done.1 = bf16[128,24,512]{2,1,0:T(8,128)(2,1)} async-done(((bf16[128,24,512]{2,1,0:T(8,128)(2,1)}), bf16[128,24,512]{2,1,0:T(8,128)(2,1)}, u32[]{:S(2)}, u32[]{:S(2)}) %all-to-all-start.1) | async-done | bytes 3145760 | tf_op jit(solution)/shard_map/all_to_all | solution.py:634
  258.2 7.2 %combine.1 = bf16[128,2048]{1,0:T(8,128)(2,1)} custom-call(bf16[3072,512]{1,0:T(8,128)(2,1)} %bitcast.8.back, s32[128,4]{1,0:T(8,128)} %copy.32.ids, f32[128,4]{1,0:T(8,128)} %copy.34.weights, f32[128,2048]{1,0:T(8,128)} %fusion.1.shared, bf16[128,2048]{1,0:T(8,128)(2,1)} %get-tuple-element.12.mixed, f32[1,2048]{1,0:T(1,128)} %bitcast.19, ...), custom_call_target="tpu_custom_call" | custom-call | flops 3000000000 | bytes 6000000 | tf_op jit(solution)/shard_map/combine/pallas_call | solution.py:611
  (11 shorter events, 0.0 us)
Async XLA Ops:
  0.0 219.6 %copy-start = (bf16[512,2048]{1,0:T(8,128)(2,1)S(1)}, bf16[512,2048]{1,0:T(8,128)(2,1)}, u32[]{:S(2)}) copy-start(bf16[512,2048]{1,0:T(8,128)(2,1)} %param.49) | copy-start | bytes 6291460
  147.4 49.5 %all-to-all-start = ((bf16[128,24,512]{2,1,0:T(8,128)(2,1)}), bf16[128,24,512]{2,1,0:T(8,128)(2,1)}, u32[]{:S(2)}, u32[]{:S(2)}) async-start(bf16[128,24,512]{2,1,0:T(8,128)(2,1)} %bitcast.15), calls=%async_computation | async-start | bytes 6291456 | tf_op jit(solution)/shard_map/all_to_all | solution.py:634
  155.8 2.7 %copy-start.2 = (bf16[2,2048,256]{2,1,0:T(8,128)(2,1)S(1)}, bf16[2,2048,256]{2,1,0:T(8,128)(2,1)}, u32[]{:S(2)}) copy-start(bf16[2,2048,256]{2,1,0:T(8,128)(2,1)} %refs_2_.1) | copy-start | bytes 6291460
  155.8 3.2 %copy-start.3 = (bf16[2,256,2048]{2,1,0:T(8,128)(2,1)S(1)}, bf16[2,256,2048]{2,1,0:T(8,128)(2,1)}, u32[]{:S(2)}) copy-start(bf16[2,256,2048]{2,1,0:T(8,128)(2,1)} %refs_3_.1) | copy-start | bytes 6291460
  157.2 3.5 %collective-permute-start = (bf16[1,2048,256]{2,1,0:T(8,128)(2,1)S(1)}, bf16[1,2048,256]{2,1,0:T(8,128)(2,1)S(1)}, u32[]{:S(2)}, u32[]{:S(2)}) collective-permute-start(bf16[1,2048,256]{2,1,0:T(8,128)(2,1)S(1)} %constant_dynamic-slice_fusion.2), channel_id=1, source_target_pairs={{0,1},{1,0},{2,3},{3,2},{4,5},{5,4},{6,7},{7,6},{8,9},{9,8},{10,11... | collective-permute-start | bytes 3145736 | tf_op jit(solution)/shard_map/ppermute | solution.py:666
  158.5 3.7 %collective-permute-start.1 = (bf16[1,2048,256]{2,1,0:T(8,128)(2,1)S(1)}, bf16[1,2048,256]{2,1,0:T(8,128)(2,1)S(1)}, u32[]{:S(2)}, u32[]{:S(2)}) collective-permute-start(bf16[1,2048,256]{2,1,0:T(8,128)(2,1)S(1)} %constant_dynamic-slice_fusion.1), channel_id=1, source_target_pairs={{0,1},{1,0},{2,3},{3,2},{4,5},{5,4},{6,7},{7,6},{8,9},{9,8},{10,11... | collective-permute-start | bytes 3145736 | tf_op jit(solution)/shard_map/ppermute | solution.py:666
  159.1 4.8 %collective-permute-start.2 = (bf16[1,256,2048]{2,1,0:T(8,128)(2,1)S(1)}, bf16[1,256,2048]{2,1,0:T(8,128)(2,1)}, u32[]{:S(2)}, u32[]{:S(2)}) collective-permute-start(bf16[1,256,2048]{2,1,0:T(8,128)(2,1)S(1)} %constant_dynamic-slice_fusion), channel_id=1, source_target_pairs={{0,1},{1,0},{2,3},{3,2},{4,5},{5,4},{6,7},{7,6},{8,9},{9,8},{10,11... | collective-permute-start | bytes 3145736 | tf_op jit(solution)/shard_map/ppermute | solution.py:666
  160.7 36.2 %copy-start.5 = (bf16[1,2048,256]{2,1,0:T(8,128)(2,1)}, bf16[1,2048,256]{2,1,0:T(8,128)(2,1)S(1)}, u32[]{:S(2)}) copy-start(bf16[1,2048,256]{2,1,0:T(8,128)(2,1)S(1)} %collective-permute-done.refs_4_) | copy-start | bytes 3145732
  162.2 1.0 copy-start.6
  211.1 5.8 %copy-start.4 = (f32[128,4]{0,1:T(4,128)S(1)}, f32[128,4]{0,1:T(4,128)}, u32[]{:S(2)}) copy-start(f32[128,4]{0,1:T(4,128)} %param.54) | copy-start | bytes 6148
  211.1 6.5 %copy-start.1 = (bf16[128,2048]{1,0:T(8,128)(2,1)S(1)}, bf16[128,2048]{1,0:T(8,128)(2,1)}, u32[]{:S(2)}) copy-start(bf16[128,2048]{1,0:T(8,128)(2,1)} %get-tuple-element.11) | copy-start | bytes 1572868
  211.1 47.1 %all-to-all-start.1 = ((bf16[128,24,512]{2,1,0:T(8,128)(2,1)}), bf16[128,24,512]{2,1,0:T(8,128)(2,1)}, u32[]{:S(2)}, u32[]{:S(2)}) async-start(bf16[128,24,512]{2,1,0:T(8,128)(2,1)} %bitcast.16), calls=%async_computation.1 | async-start | bytes 6291456 | tf_op jit(solution)/shard_map/all_to_all | solution.py:634

commit v3 on v2

--- a/solution.py
+++ b/solution.py
@@ -24,6 +24,8 @@
 ATTN_BYTES = 60 * 2**20
 VMEM_BYTES = 60 * 2**20
 MESH = pl.DeviceIdType.MESH
+VMEM = pl.BlockSpec(memory_space=pltpu.VMEM)
+HBM = pl.BlockSpec(memory_space=pltpu.HBM)
 ORDERS = ((0, 1, 2), (1, 2, 0), (2, 0, 1))
 STRIDE = (1, 4, 16)
 
@@ -425,43 +427,55 @@
 
 
 def ranks(ids):
-    lane = lax.broadcasted_iota(jnp.int32, (TQ, EXPERTS), 1)
-    named = jnp.zeros((TQ, EXPERTS), jnp.float32)
+    expert = lax.broadcasted_iota(jnp.int32, (EXPERTS, TQ), 0)
+    named = jnp.zeros((EXPERTS, TQ), jnp.float32)
     for k in range(TOPK):
-        named = named + (ids[:, k : k + 1] == lane).astype(jnp.float32)
-    below = lax.broadcasted_iota(jnp.int32, (TQ, TQ), 1) < lax.broadcasted_iota(
-        jnp.int32, (TQ, TQ), 0
-    )
-    count = dot(below.astype(jnp.bfloat16), named.astype(jnp.bfloat16))
+        named = named + (ids[k : k + 1, :] == expert).astype(jnp.float32)
+    before = lax.broadcasted_iota(jnp.int32, (TQ, TQ), 0) < lax.broadcasted_iota(
+        jnp.int32, (TQ, TQ), 1
+    )
+    count = dot(named.astype(jnp.bfloat16), before.astype(jnp.bfloat16))
     return (named * (count + 1.0)).astype(jnp.bfloat16)
 
 
 def mid_kernel(
-    f, on, ow, stream, gmix, gffn, ids, rank_of, piece_mask, mixed_out, normed_out, slab
+    f, on_in, ow_in, stream, gmix, gffn, ids, rank_of, piece_mask, mixed_out, normed_out, slab,
+    on, ow, picks, sems,
 ):
-    projected = (
-        dot(f[0, :, 0:512], on[0:512, :])
-        + dot(f[1, :, 0:512], on[512:1024, :])
-        + dot(f[0, :, 512:1024], ow[0:512, :])
-        + dot(f[1, :, 512:1024], ow[512:1024, :])
-    )
-    mixed = (stream[...].astype(jnp.float32) + rms(projected, gmix[...])).astype(jnp.bfloat16)
-    mixed_out[...] = mixed
-    normed = rms(mixed.astype(jnp.float32), gffn[...]).astype(jnp.bfloat16)
-    normed_out[...] = normed
-    stacked = jnp.concatenate([normed[:, c * WIDTH : (c + 1) * WIDTH] for c in range(PIECES)], 0)
+    loads = []
+    for i, (src, dst) in enumerate(((on_in, on), (ow_in, ow))):
+        copy = pltpu.make_async_copy(src, dst, sems.at[i])
+        copy.start()
+        loads.append(copy)
     value = ranks(ids[...])
     row = lax.broadcasted_iota(jnp.int32, (GROUP_ROWS, EXPERTS), 0)
     lane = lax.broadcasted_iota(jnp.int32, (GROUP_ROWS, EXPERTS), 1)
     for g in range(EXPERTS // GROUP):
         low = (lane - g * GROUP) * SLAB
         spread = ((row >= low) & (row < low + SLAB)).astype(jnp.bfloat16)
-        here = lax.dot_general(
-            spread, value, (((1,), (1,)), ((), ())), preferred_element_type=jnp.float32
-        )
-        chosen = (here == rank_of[...]).astype(jnp.float32).astype(jnp.bfloat16)
+        chosen = (dot(spread, value) == rank_of[...]).astype(jnp.float32).astype(jnp.bfloat16)
         chosen = jnp.concatenate([chosen] * PIECES, axis=1) * piece_mask[...]
-        slab[g * GROUP_ROWS : (g + 1) * GROUP_ROWS, :] = dot(chosen, stacked).astype(jnp.bfloat16)
+        picks[g * GROUP_ROWS : (g + 1) * GROUP_ROWS, :] = chosen
+    for copy in loads:
+        copy.wait()
+    projected = (
+        dot(f[0, :, 0:512], on[0:512, :])
+        + dot(f[1, :, 0:512], on[512:1024, :])
+        + dot(f[0, :, 512:1024], ow[0:512, :])
+        + dot(f[1, :, 512:1024], ow[512:1024, :])
+    )
+    mixed = (stream[...].astype(jnp.float32) + rms(projected, gmix[...])).astype(jnp.bfloat16)
+    mixed_out[...] = mixed
+    normed = rms(mixed.astype(jnp.float32), gffn[...]).astype(jnp.bfloat16)
+    normed_out[...] = normed
+    stacked = jnp.concatenate([normed[:, c * WIDTH : (c + 1) * WIDTH] for c in range(PIECES)], 0)
+
+    def place_rows(g, carry):
+        part = pl.ds(pl.multiple_of(g * GROUP_ROWS, GROUP_ROWS), GROUP_ROWS)
+        slab[part, :] = dot(picks[part, :], stacked).astype(jnp.bfloat16)
+        return carry
+
+    lax.fori_loop(0, EXPERTS // GROUP, place_rows, 0, unroll=4)
 
 
 def slab_tables():
@@ -483,6 +497,13 @@
     rank, piece = slab_tables()
     return pl.pallas_call(
         mid_kernel,
+        in_specs=[VMEM, HBM, HBM, *[VMEM] * 6],
+        scratch_shapes=[
+            pltpu.VMEM((D // 2, D), jnp.bfloat16),
+            pltpu.VMEM((D // 2, D), jnp.bfloat16),
+            pltpu.VMEM((EXPERTS * SLAB, PIECES * TQ), jnp.bfloat16),
+            pltpu.SemaphoreType.DMA((2,)),
+        ],
         out_shape=(
             jax.ShapeDtypeStruct((TQ, D), jnp.bfloat16),
             jax.ShapeDtypeStruct((TQ, D), jnp.bfloat16),
@@ -504,7 +525,24 @@
     )
 
 
-def expert_kernel(x, g1, u1, d1, g2, u2, d2, order, order_t, out, rows, results):
+def expert_kernel(
+    which, x, g1_in, u1_in, d1_in, g2_in, u2_in, d2_in, order, order_t, out,
+    rows, results, g1, u1, d1, g2, u2, d2, sems,
+):
+    loads = []
+    for i, (src, dst) in enumerate(
+        (
+            (g1_in.at[which[0]], g1),
+            (u1_in.at[which[0]], u1),
+            (d1_in.at[which[0]], d1),
+            (g2_in.at[0], g2),
+            (u2_in.at[0], u2),
+            (d2_in.at[0], d2),
+        )
+    ):
+        copy = pltpu.make_async_copy(src, dst, sems.at[i])
+        copy.start()
+        loads.append(copy)
     span = GROUP * CAP
     for g in range(EXPERTS // GROUP):
         got = dot(order[...], x[g * GROUP_ROWS : (g + 1) * GROUP_ROWS, :]).astype(jnp.bfloat16)
@@ -512,46 +550,42 @@
             rows[g * span : (g + 1) * span, c * WIDTH : (c + 1) * WIDTH] = got[
                 c * span : (c + 1) * span, :
             ]
+    for copy in loads:
+        copy.wait()
     for m in range(0, EXPERTS * CAP, 256):
         part = rows[m : m + 256, :]
         total = None
         for gate, up, down in ((g1, u1, d1), (g2, u2, d2)):
-            gated = dot(part, gate[0])
-            hidden = (gated / (1.0 + jnp.exp(-gated)) * dot(part, up[0])).astype(jnp.bfloat16)
-            term = dot(hidden, down[0])
+            gated = dot(part, gate[...])
+            hidden = (gated / (1.0 + jnp.exp(-gated)) * dot(part, up[...])).astype(jnp.bfloat16)
+            term = dot(hidden, down[...])
             total = term if total is None else total + term
         results[m : m + 256, :] = total.astype(jnp.bfloat16)
-    for g in range(EXPERTS // GROUP):
+
+    def give_back(g, carry):
+        base = pl.multiple_of(g * span, span)
         stacked = jnp.concatenate(
-            [
-                results[g * span : (g + 1) * span, c * WIDTH : (c + 1) * WIDTH]
-                for c in range(PIECES)
-            ],
-            0,
+            [results[pl.ds(base, span), c * WIDTH : (c + 1) * WIDTH] for c in range(PIECES)], 0
         )
-        out[g * GROUP_ROWS : (g + 1) * GROUP_ROWS, :] = dot(order_t[...], stacked).astype(
-            jnp.bfloat16
-        )
+        part = pl.ds(pl.multiple_of(g * GROUP_ROWS, GROUP_ROWS), GROUP_ROWS)
+        out[part, :] = dot(order_t[...], stacked).astype(jnp.bfloat16)
+        return carry
+
+    lax.fori_loop(0, EXPERTS // GROUP, give_back, 0, unroll=4)
 
 
 def run_expert(which, x, gate, up, down, gate2, up2, down2):
     table = order_table()
     full = lambda *shape: pl.BlockSpec(shape, lambda i, w: (0,) * len(shape))
-    mine = lambda *shape: pl.BlockSpec((1, *shape), lambda i, w: (w[0], 0, 0))
     half = gate.shape[2]
     return pl.pallas_call(
-        expert_kernel_with_prefetch,
+        expert_kernel,
         grid_spec=pltpu.PrefetchScalarGridSpec(
             num_scalar_prefetch=1,
             grid=(1,),
             in_specs=[
                 full(EXPERTS * SLAB, WIDTH),
-                mine(D, half),
-                mine(D, half),
-                mine(half, D),
-                full(1, D, half),
-                full(1, D, half),
-                full(1, half, D),
+                *[HBM] * 6,
                 full(GROUP_ROWS, GROUP_ROWS),
                 full(GROUP_ROWS, GROUP_ROWS),
             ],
@@ -559,6 +593,11 @@
             scratch_shapes=[
                 pltpu.VMEM((EXPERTS * CAP, D), jnp.bfloat16),
                 pltpu.VMEM((EXPERTS * CAP, D), jnp.bfloat16),
+                *[
+                    pltpu.VMEM(shape, jnp.bfloat16)
+                    for shape in ((D, half), (D, half), (half, D)) * 2
+                ],
+                pltpu.SemaphoreType.DMA((6,)),
             ],
         ),
         out_shape=jax.ShapeDtypeStruct((EXPERTS * SLAB, WIDTH), jnp.bfloat16),
@@ -579,17 +618,22 @@
     )
 
 
-def expert_kernel_with_prefetch(which, *refs):
-    expert_kernel(*refs)
-
-
-def combine_kernel(back, ids, weights, shared, mixed, gpost, rank_row, piece_row, out):
+def combine_kernel(
+    back_in, ids, weights, shared, mixed, gpost, rank_row, piece_row, out, back, sems
+):
+    loads = []
+    for g in range(EXPERTS // GROUP):
+        part = pl.ds(g * GROUP_ROWS, GROUP_ROWS)
+        copy = pltpu.make_async_copy(back_in.at[part, :], back.at[part, :], sems.at[g])
+        copy.start()
+        loads.append(copy)
     value = ranks(ids[...])
-    lane = lax.broadcasted_iota(jnp.int32, (TQ, EXPERTS), 1)
-    share = jnp.zeros((TQ, EXPERTS), jnp.float32)
+    expert = lax.broadcasted_iota(jnp.int32, (EXPERTS, TQ), 0)
+    share = jnp.zeros((EXPERTS, TQ), jnp.float32)
     for k in range(TOPK):
-        share = share + jnp.where(ids[:, k : k + 1] == lane, weights[:, k : k + 1], 0.0)
-    share = share.astype(jnp.bfloat16)
+        share = share + jnp.where(ids[k : k + 1, :] == expert, weights[k : k + 1, :], 0.0)
+    value = value.astype(jnp.float32).T.astype(jnp.bfloat16)
+    share = share.T.astype(jnp.bfloat16)
     row = lax.broadcasted_iota(jnp.int32, (EXPERTS, GROUP_ROWS), 0)
     col = lax.broadcasted_iota(jnp.int32, (EXPERTS, GROUP_ROWS), 1)
     total = jnp.zeros((PIECES * TQ, WIDTH), jnp.float32)
@@ -600,6 +644,7 @@
         picks = jnp.concatenate(
             [jnp.where(piece_row[...] == float(c), held, 0.0) for c in range(PIECES)], 0
         ).astype(jnp.bfloat16)
+        loads[g].wait()
         total = total + dot(picks, back[g * GROUP_ROWS : (g + 1) * GROUP_ROWS, :])
     routed = jnp.concatenate([total[c * TQ : (c + 1) * TQ, :] for c in range(PIECES)], axis=1)
     combined = shared[...] + routed
@@ -610,6 +655,11 @@
     i = np.arange(GROUP_ROWS) % SLAB
     return pl.pallas_call(
         combine_kernel,
+        in_specs=[HBM, *[VMEM] * 7],
+        scratch_shapes=[
+            pltpu.VMEM((EXPERTS * SLAB, WIDTH), jnp.bfloat16),
+            pltpu.SemaphoreType.DMA((EXPERTS // GROUP,)),
+        ],
         out_shape=jax.ShapeDtypeStruct((TQ, D), jnp.bfloat16),
         compiler_params=pltpu.CompilerParams(vmem_limit_bytes=VMEM_BYTES),
         cost_estimate=pl.CostEstimate(flops=3 * 10**9, bytes_accessed=6 * 10**6, transcendentals=0),
@@ -679,7 +729,7 @@
         gain_wide,
     )
     mixed, normed, slab = mid(
-        attended, out_narrow, out_wide, stream, gain_mix, gain_ffn, expert_ids
+        attended, out_narrow, out_wide, stream, gain_mix, gain_ffn, expert_ids.T
     )
     incoming = exchanged(slab)
     results = run_expert(
@@ -695,7 +745,7 @@
         jax.nn.silu(dot(normed, shared_gate)) * dot(normed, shared_up)
     ).astype(jnp.bfloat16)
     shared_out = dot(shared_hidden, shared_down)
-    return combine(back, expert_ids, route_weights, shared_out, mixed, gain_post)
+    return combine(back, expert_ids.T, route_weights.T, shared_out, mixed, gain_post)
 
 
 def solution(mesh):

time: 266 us -> 265 us (level)
  no operation moved by 1% of the time
where the time goes in v3:
time: 265 us; the launch traced here: 264 us
  Pallas kernels  167 us (63%)
  waiting for transfers between devices  71.9 us (27%)
  starting transfers between devices  16.6 us (6%)
  matrix products  5.47 us (2%)
  local copies, waits for them, and re-layouts  2.65 us (1%)
    pallas_call x1, Pallas kernels, attention(): pl.pallas_call(attn_kernel, in_specs=[vmem, vmem, hbm, hbm, hbm, hbm, sme...  136 us
    all_to_all x2, waiting for transfers between devices, exchanged(): lax.all_to_all(pieces, BOTH, 0, 0, tiled=True)  68.7 us
    all_to_all x2, starting transfers between devices, exchanged(): lax.all_to_all(pieces, BOTH, 0, 0, tiled=True)  14.2 us
    pallas_call x1, Pallas kernels, run_expert(): pl.pallas_call(expert_kernel, grid_spec=pltpu.PrefetchScalarGridSpec(num_...  13.8 us
    pallas_call x1, Pallas kernels, mid(): pl.pallas_call(mid_kernel, in_specs=[VMEM, HBM, HBM, *[VMEM] * 6], scratc...  10.2 us
    pallas_call x1, Pallas kernels, combine(): pl.pallas_call(combine_kernel, in_specs=[HBM, *[VMEM] * 7], scratch_shape...  7.45 us
    dot_general x2, matrix products, dot(): return jnp.dot(a, b, preferred_element_type=jnp.float32)  5.47 us
  transfers between devices with their start and end apart: 5, of which 5 were waited for; matrix products, arithmetic and copies ran while one was open for 3% of the time, Pallas kernels for 0%

profile of v3, /device:TPU:1, one launch (start us, length us, event | category | flops | bytes accessed | tf_op | source)
XLA Modules:
  0.0 264.3 jit_solution(3545460097911313080)
XLA Ops:
  0.0 0.0 copy-start
  0.0 136.0 %attention.1 = (bf16[4,4,4,256,768]{4,3,2,1,0:T(8,128)(2,1)}, bf16[2,128,1024]{2,1,0:T(8,128)(2,1)}) custom-call(bf16[256,512]{1,0:T(8,128)(2,1)} %qn_in.1, bf16[256,512]{1,0:T(8,128)(2,1)} %qw_in.1, bf16[256,128]{1,0:T(8,128)(2,1)} %kn_in.1, bf16[256,128]{1,0:T(8,128)(2,1)} %vn_in.1, bf16[256,256]{1,0:T(8,128)(2,1)} %kw_in.1, bf16[256,256]{1,0:T(8,128)(2,1)} %vw_in.1, ...), custom_call_target="tpu_custom_call" | custom-call | flops 30000001024 | bytes 60000000 | tf_op jit(solution)/shard_map/attention/pallas_call | solution.py:375
  136.0 10.2 %mid.1 = (bf16[128,2048]{1,0:T(8,128)(2,1)}, bf16[128,2048]{1,0:T(8,128)(2,1)}, bf16[3072,512]{1,0:T(8,128)(2,1)}) custom-call(bf16[2,128,1024]{2,1,0:T(8,128)(2,1)} %get-tuple-element.9.f, bf16[1024,2048]{1,0:T(8,128)(2,1)} %on_in.1, bf16[1024,2048]{1,0:T(8,128)(2,1)} %ow_in.1, bf16[128,2048]{1,0:T(8,128)(2,1)} %stream.1, f32[1,2048]{1,0:T(1,128)} %bitcast.19, ...), custom_call_target="tpu_custom_call" | custom-call | flops 4000000000 | bytes 14000000 | tf_op jit(solution)/shard_map/mid/pallas_call | solution.py:498
  146.2 8.4 %all-to-all-start = ((bf16[128,24,512]{2,1,0:T(8,128)(2,1)}), bf16[128,24,512]{2,1,0:T(8,128)(2,1)}, u32[]{:S(2)}, u32[]{:S(2)}) async-start(bf16[128,24,512]{2,1,0:T(8,128)(2,1)} %bitcast.17), calls=%async_computation | async-start | bytes 6291456 | tf_op jit(solution)/shard_map/all_to_all | solution.py:684
  154.6 0.0 copy-start.2
  154.6 0.0 copy-start.3
  154.6 1.4 constant_dynamic-slice_fusion.2
  156.0 1.4 collective-permute-start
  157.4 0.1 constant_dynamic-slice_fusion.1
  157.5 0.4 collective-permute-start.1
  157.9 0.1 constant_dynamic-slice_fusion
  158.0 0.6 collective-permute-start.2
  158.6 1.1 collective-permute-done.g2_in
  159.7 1.5 collective-permute-done.1.u2_in
  161.2 1.0 copy-done.5
  162.2 0.6 collective-permute-done.2.d2_in
  162.8 32.9 %all-to-all-done = bf16[128,24,512]{2,1,0:T(8,128)(2,1)} async-done(((bf16[128,24,512]{2,1,0:T(8,128)(2,1)}), bf16[128,24,512]{2,1,0:T(8,128)(2,1)}, u32[]{:S(2)}, u32[]{:S(2)}) %all-to-all-start) | async-done | bytes 3145760 | tf_op jit(solution)/shard_map/all_to_all | solution.py:684
  195.7 13.8 %expert.1 = bf16[3072,512]{1,0:T(8,128)(2,1)} custom-call(s32[1]{0:T(128)} %bitcast.which, bf16[3072,512]{1,0:T(8,128)(2,1)} %bitcast.7.x, bf16[2,2048,256]{2,1,0:T(8,128)(2,1)} %g1_in.1, bf16[2,2048,256]{2,1,0:T(8,128)(2,1)} %u1_in.1, bf16[2,256,2048]{2,1,0:T(8,128)(2,1)} %d1_in.1, bf16[1,2048,256]{2,1,0:T(8,128)(2,1)} %copy-done.4, ...), custom_call_target="tpu_custom_call" | custom-call | flops 6000000000 | bytes 14000000 | tf_op jit(solution)/shard_map/expert/pallas_call | solution.py:581
  209.6 0.0 copy-start.1
  209.6 5.8 %all-to-all-start.1 = ((bf16[128,24,512]{2,1,0:T(8,128)(2,1)}), bf16[128,24,512]{2,1,0:T(8,128)(2,1)}, u32[]{:S(2)}, u32[]{:S(2)}) async-start(bf16[128,24,512]{2,1,0:T(8,128)(2,1)} %bitcast.18), calls=%async_computation.1 | async-start | bytes 6291456 | tf_op jit(solution)/shard_map/all_to_all | solution.py:684
  215.4 2.0 fusion.9
  217.5 3.4 %fusion.1.shared = f32[128,2048]{1,0:T(8,128)} fusion(bf16[512,2048]{1,0:T(8,128)(2,1)S(1)} %copy-done, bf16[128,2048]{1,0:T(8,128)(2,1)S(1)} %copy-done.1, bf16[2048,512]{1,0:T(8,128)(2,1)} %param.48, f32[128,512]{1,0:T(8,128)S(1)} %fusion.9), kind=kOutput, calls=%fused_computation.2 | convolution fusion | flops 537264128 | bytes 6029312 | tf_op jit(solution)/shard_map/dot_general | solution.py:426
  220.9 35.8 %all-to-all-done.1 = bf16[128,24,512]{2,1,0:T(8,128)(2,1)} async-done(((bf16[128,24,512]{2,1,0:T(8,128)(2,1)}), bf16[128,24,512]{2,1,0:T(8,128)(2,1)}, u32[]{:S(2)}, u32[]{:S(2)}) %all-to-all-start.1) | async-done | bytes 3145760 | tf_op jit(solution)/shard_map/all_to_all | solution.py:684
  256.7 7.5 %combine.1 = bf16[128,2048]{1,0:T(8,128)(2,1)} custom-call(bf16[3072,512]{1,0:T(8,128)(2,1)} %bitcast.9.back_in, s32[4,128]{1,0:T(4,128)} %bitcast.23, f32[4,128]{1,0:T(4,128)} %bitcast.24, f32[128,2048]{1,0:T(8,128)} %fusion.1.shared, bf16[128,2048]{1,0:T(8,128)(2,1)} %get-tuple-element.12.mixed, f32[1,2048]{1,0:T(1,128)} %bitcast.21, ...), custom_call_target="tpu_custom_call" | custom-call | flops 3000000000 | bytes 6000000 | tf_op jit(solution)/shard_map/combine/pallas_call | solution.py:656
  (7 shorter events, 0.0 us)
Async XLA Ops:
  0.0 217.5 %copy-start = (bf16[512,2048]{1,0:T(8,128)(2,1)S(1)}, bf16[512,2048]{1,0:T(8,128)(2,1)}, u32[]{:S(2)}) copy-start(bf16[512,2048]{1,0:T(8,128)(2,1)} %param.49) | copy-start | bytes 6291460
  146.2 49.6 %all-to-all-start = ((bf16[128,24,512]{2,1,0:T(8,128)(2,1)}), bf16[128,24,512]{2,1,0:T(8,128)(2,1)}, u32[]{:S(2)}, u32[]{:S(2)}) async-start(bf16[128,24,512]{2,1,0:T(8,128)(2,1)} %bitcast.17), calls=%async_computation | async-start | bytes 6291456 | tf_op jit(solution)/shard_map/all_to_all | solution.py:684
  154.6 2.9 %copy-start.2 = (bf16[2,2048,256]{2,1,0:T(8,128)(2,1)S(1)}, bf16[2,2048,256]{2,1,0:T(8,128)(2,1)}, u32[]{:S(2)}) copy-start(bf16[2,2048,256]{2,1,0:T(8,128)(2,1)} %u1_in.1) | copy-start | bytes 6291460
  154.6 3.4 %copy-start.3 = (bf16[2,256,2048]{2,1,0:T(8,128)(2,1)S(1)}, bf16[2,256,2048]{2,1,0:T(8,128)(2,1)}, u32[]{:S(2)}) copy-start(bf16[2,256,2048]{2,1,0:T(8,128)(2,1)} %d1_in.1) | copy-start | bytes 6291460
  156.0 3.7 %collective-permute-start = (bf16[1,2048,256]{2,1,0:T(8,128)(2,1)S(1)}, bf16[1,2048,256]{2,1,0:T(8,128)(2,1)S(1)}, u32[]{:S(2)}, u32[]{:S(2)}) collective-permute-start(bf16[1,2048,256]{2,1,0:T(8,128)(2,1)S(1)} %constant_dynamic-slice_fusion.2), channel_id=1, source_target_pairs={{0,1},{1,0},{2,3},{3,2},{4,5},{5,4},{6,7},{7,6},{8,9},{9,8},{10,11... | collective-permute-start | bytes 3145736 | tf_op jit(solution)/shard_map/ppermute | solution.py:716
  157.5 3.7 %collective-permute-start.1 = (bf16[1,2048,256]{2,1,0:T(8,128)(2,1)S(1)}, bf16[1,2048,256]{2,1,0:T(8,128)(2,1)S(1)}, u32[]{:S(2)}, u32[]{:S(2)}) collective-permute-start(bf16[1,2048,256]{2,1,0:T(8,128)(2,1)S(1)} %constant_dynamic-slice_fusion.1), channel_id=1, source_target_pairs={{0,1},{1,0},{2,3},{3,2},{4,5},{5,4},{6,7},{7,6},{8,9},{9,8},{10,11... | collective-permute-start | bytes 3145736 | tf_op jit(solution)/shard_map/ppermute | solution.py:716
  158.0 4.8 %collective-permute-start.2 = (bf16[1,256,2048]{2,1,0:T(8,128)(2,1)S(1)}, bf16[1,256,2048]{2,1,0:T(8,128)(2,1)}, u32[]{:S(2)}, u32[]{:S(2)}) collective-permute-start(bf16[1,256,2048]{2,1,0:T(8,128)(2,1)S(1)} %constant_dynamic-slice_fusion), channel_id=1, source_target_pairs={{0,1},{1,0},{2,3},{3,2},{4,5},{5,4},{6,7},{7,6},{8,9},{9,8},{10,11... | collective-permute-start | bytes 3145736 | tf_op jit(solution)/shard_map/ppermute | solution.py:716
  159.7 36.0 %copy-start.4 = (bf16[1,2048,256]{2,1,0:T(8,128)(2,1)}, bf16[1,2048,256]{2,1,0:T(8,128)(2,1)S(1)}, u32[]{:S(2)}) copy-start(bf16[1,2048,256]{2,1,0:T(8,128)(2,1)S(1)} %collective-permute-done.g2_in) | copy-start | bytes 3145732
  161.2 1.0 copy-start.5
  209.6 5.8 %copy-start.1 = (bf16[128,2048]{1,0:T(8,128)(2,1)S(1)}, bf16[128,2048]{1,0:T(8,128)(2,1)}, u32[]{:S(2)}) copy-start(bf16[128,2048]{1,0:T(8,128)(2,1)} %get-tuple-element.11) | copy-start | bytes 1572868
  209.6 47.1 %all-to-all-start.1 = ((bf16[128,24,512]{2,1,0:T(8,128)(2,1)}), bf16[128,24,512]{2,1,0:T(8,128)(2,1)}, u32[]{:S(2)}, u32[]{:S(2)}) async-start(bf16[128,24,512]{2,1,0:T(8,128)(2,1)} %bitcast.18), calls=%async_computation.1 | async-start | bytes 6291456 | tf_op jit(solution)/shard_map/all_to_all | solution.py:684

commit v4 on v3

--- a/solution.py
+++ b/solution.py
@@ -239,7 +239,14 @@
             @pl.when(s == STARTS[chunk])
             def _():
                 end(2, *CHUNKS[chunk], chunk)
-                fetch(s, slot)
+        opening = s == STARTS[0]
+        for start in STARTS[1:]:
+            opening = opening | (s == start)
+
+        @pl.when(opening)
+        def _():
+            fetch(s, slot)
+
         for chunk, turn in TURNS.items():
             @pl.when(s == turn)
             def _():
@@ -475,7 +482,7 @@
         slab[part, :] = dot(picks[part, :], stacked).astype(jnp.bfloat16)
         return carry
 
-    lax.fori_loop(0, EXPERTS // GROUP, place_rows, 0, unroll=4)
+    lax.fori_loop(0, EXPERTS // GROUP, place_rows, 0, unroll=8)
 
 
 def slab_tables():
@@ -571,7 +578,7 @@
         out[part, :] = dot(order_t[...], stacked).astype(jnp.bfloat16)
         return carry
 
-    lax.fori_loop(0, EXPERTS // GROUP, give_back, 0, unroll=4)
+    lax.fori_loop(0, EXPERTS // GROUP, give_back, 0, unroll=8)
 
 
 def run_expert(which, x, gate, up, down, gate2, up2, down2):

time: 265 us -> 265 us (level)
  no operation moved by 1% of the time
where the time goes in v4:
time: 265 us; the launch traced here: 264 us
  Pallas kernels  167 us (63%)
  waiting for transfers between devices  72.1 us (27%)
  starting transfers between devices  16.6 us (6%)
  matrix products  5.47 us (2%)
  local copies, waits for them, and re-layouts  2.65 us (1%)
    pallas_call x1, Pallas kernels, attention(): pl.pallas_call(attn_kernel, in_specs=[vmem, vmem, hbm, hbm, hbm, hbm, sme...  136 us
    all_to_all x2, waiting for transfers between devices, exchanged(): lax.all_to_all(pieces, BOTH, 0, 0, tiled=True)  68.9 us
    all_to_all x2, starting transfers between devices, exchanged(): lax.all_to_all(pieces, BOTH, 0, 0, tiled=True)  14.4 us
    pallas_call x1, Pallas kernels, run_expert(): pl.pallas_call(expert_kernel, grid_spec=pltpu.PrefetchScalarGridSpec(num_...  13.5 us
    pallas_call x1, Pallas kernels, mid(): pl.pallas_call(mid_kernel, in_specs=[VMEM, HBM, HBM, *[VMEM] * 6], scratc...  10 us
    pallas_call x1, Pallas kernels, combine(): pl.pallas_call(combine_kernel, in_specs=[HBM, *[VMEM] * 7], scratch_shape...  7.45 us
    dot_general x2, matrix products, dot(): return jnp.dot(a, b, preferred_element_type=jnp.float32)  5.47 us
  transfers between devices with their start and end apart: 5, of which 5 were waited for; matrix products, arithmetic and copies ran while one was open for 3% of the time, Pallas kernels for 0%

profile of v4, /device:TPU:1, one launch (start us, length us, event | category | flops | bytes accessed | tf_op | source)
XLA Modules:
  0.0 264.3 jit_solution(7021017814598477382)
XLA Ops:
  0.0 136.3 %attention.1 = (bf16[4,4,4,256,768]{4,3,2,1,0:T(8,128)(2,1)}, bf16[2,128,1024]{2,1,0:T(8,128)(2,1)}) custom-call(bf16[256,512]{1,0:T(8,128)(2,1)} %qn_in.1, bf16[256,512]{1,0:T(8,128)(2,1)} %qw_in.1, bf16[256,128]{1,0:T(8,128)(2,1)} %kn_in.1, bf16[256,128]{1,0:T(8,128)(2,1)} %vn_in.1, bf16[256,256]{1,0:T(8,128)(2,1)} %kw_in.1, bf16[256,256]{1,0:T(8,128)(2,1)} %vw_in.1, ...), custom_call_target="tpu_custom_call" | custom-call | flops 30000001024 | bytes 60000000 | tf_op jit(solution)/shard_map/attention/pallas_call | solution.py:382
  136.3 10.0 %mid.1 = (bf16[128,2048]{1,0:T(8,128)(2,1)}, bf16[128,2048]{1,0:T(8,128)(2,1)}, bf16[3072,512]{1,0:T(8,128)(2,1)}) custom-call(bf16[2,128,1024]{2,1,0:T(8,128)(2,1)} %get-tuple-element.9.f, bf16[1024,2048]{1,0:T(8,128)(2,1)} %on_in.1, bf16[1024,2048]{1,0:T(8,128)(2,1)} %ow_in.1, bf16[128,2048]{1,0:T(8,128)(2,1)} %stream.1, f32[1,2048]{1,0:T(1,128)} %bitcast.19, ...), custom_call_target="tpu_custom_call" | custom-call | flops 4000000000 | bytes 14000000 | tf_op jit(solution)/shard_map/mid/pallas_call | solution.py:505
  146.3 8.5 %all-to-all-start = ((bf16[128,24,512]{2,1,0:T(8,128)(2,1)}), bf16[128,24,512]{2,1,0:T(8,128)(2,1)}, u32[]{:S(2)}, u32[]{:S(2)}) async-start(bf16[128,24,512]{2,1,0:T(8,128)(2,1)} %bitcast.17), calls=%async_computation | async-start | bytes 6291456 | tf_op jit(solution)/shard_map/all_to_all | solution.py:691
  154.8 0.0 copy-start.2
  154.9 0.0 copy-start.3
  154.9 1.4 constant_dynamic-slice_fusion.2
  156.3 1.2 collective-permute-start
  157.5 0.1 constant_dynamic-slice_fusion.1
  157.6 0.4 collective-permute-start.1
  158.0 0.1 constant_dynamic-slice_fusion
  158.2 0.6 collective-permute-start.2
  158.7 1.1 collective-permute-done.g2_in
  159.8 1.5 collective-permute-done.1.u2_in
  161.3 1.0 copy-done.5
  162.3 0.6 collective-permute-done.2.d2_in
  163.0 33.1 %all-to-all-done = bf16[128,24,512]{2,1,0:T(8,128)(2,1)} async-done(((bf16[128,24,512]{2,1,0:T(8,128)(2,1)}), bf16[128,24,512]{2,1,0:T(8,128)(2,1)}, u32[]{:S(2)}, u32[]{:S(2)}) %all-to-all-start) | async-done | bytes 3145760 | tf_op jit(solution)/shard_map/all_to_all | solution.py:691
  196.0 0.0 copy-done.4
  196.0 13.5 %expert.1 = bf16[3072,512]{1,0:T(8,128)(2,1)} custom-call(s32[1]{0:T(128)} %bitcast.which, bf16[3072,512]{1,0:T(8,128)(2,1)} %bitcast.7.x, bf16[2,2048,256]{2,1,0:T(8,128)(2,1)} %g1_in.1, bf16[2,2048,256]{2,1,0:T(8,128)(2,1)} %u1_in.1, bf16[2,256,2048]{2,1,0:T(8,128)(2,1)} %d1_in.1, bf16[1,2048,256]{2,1,0:T(8,128)(2,1)} %copy-done.4, ...), custom_call_target="tpu_custom_call" | custom-call | flops 6000000000 | bytes 14000000 | tf_op jit(solution)/shard_map/expert/pallas_call | solution.py:588
  209.5 0.0 copy-start.1
  209.5 5.8 %all-to-all-start.1 = ((bf16[128,24,512]{2,1,0:T(8,128)(2,1)}), bf16[128,24,512]{2,1,0:T(8,128)(2,1)}, u32[]{:S(2)}, u32[]{:S(2)}) async-start(bf16[128,24,512]{2,1,0:T(8,128)(2,1)} %bitcast.18), calls=%async_computation.1 | async-start | bytes 6291456 | tf_op jit(solution)/shard_map/all_to_all | solution.py:691
  215.4 2.0 fusion.9
  217.4 3.4 %fusion.1.shared = f32[128,2048]{1,0:T(8,128)} fusion(bf16[512,2048]{1,0:T(8,128)(2,1)S(1)} %copy-done, bf16[128,2048]{1,0:T(8,128)(2,1)S(1)} %copy-done.1, bf16[2048,512]{1,0:T(8,128)(2,1)} %param.48, f32[128,512]{1,0:T(8,128)S(1)} %fusion.9), kind=kOutput, calls=%fused_computation.2 | convolution fusion | flops 537264128 | bytes 6029312 | tf_op jit(solution)/shard_map/dot_general | solution.py:433
  220.9 35.8 %all-to-all-done.1 = bf16[128,24,512]{2,1,0:T(8,128)(2,1)} async-done(((bf16[128,24,512]{2,1,0:T(8,128)(2,1)}), bf16[128,24,512]{2,1,0:T(8,128)(2,1)}, u32[]{:S(2)}, u32[]{:S(2)}) %all-to-all-start.1) | async-done | bytes 3145760 | tf_op jit(solution)/shard_map/all_to_all | solution.py:691
  256.7 7.5 %combine.1 = bf16[128,2048]{1,0:T(8,128)(2,1)} custom-call(bf16[3072,512]{1,0:T(8,128)(2,1)} %bitcast.9.back_in, s32[4,128]{1,0:T(4,128)} %bitcast.23, f32[4,128]{1,0:T(4,128)} %bitcast.24, f32[128,2048]{1,0:T(8,128)} %fusion.1.shared, bf16[128,2048]{1,0:T(8,128)(2,1)} %get-tuple-element.12.mixed, f32[1,2048]{1,0:T(1,128)} %bitcast.21, ...), custom_call_target="tpu_custom_call" | custom-call | flops 3000000000 | bytes 6000000 | tf_op jit(solution)/shard_map/combine/pallas_call | solution.py:663
  (7 shorter events, 0.0 us)
Async XLA Ops:
  0.0 217.4 %copy-start = (bf16[512,2048]{1,0:T(8,128)(2,1)S(1)}, bf16[512,2048]{1,0:T(8,128)(2,1)}, u32[]{:S(2)}) copy-start(bf16[512,2048]{1,0:T(8,128)(2,1)} %param.49) | copy-start | bytes 6291460
  146.3 49.7 %all-to-all-start = ((bf16[128,24,512]{2,1,0:T(8,128)(2,1)}), bf16[128,24,512]{2,1,0:T(8,128)(2,1)}, u32[]{:S(2)}, u32[]{:S(2)}) async-start(bf16[128,24,512]{2,1,0:T(8,128)(2,1)} %bitcast.17), calls=%async_computation | async-start | bytes 6291456 | tf_op jit(solution)/shard_map/all_to_all | solution.py:691
  154.8 2.7 %copy-start.2 = (bf16[2,2048,256]{2,1,0:T(8,128)(2,1)S(1)}, bf16[2,2048,256]{2,1,0:T(8,128)(2,1)}, u32[]{:S(2)}) copy-start(bf16[2,2048,256]{2,1,0:T(8,128)(2,1)} %u1_in.1) | copy-start | bytes 6291460
  154.9 3.2 %copy-start.3 = (bf16[2,256,2048]{2,1,0:T(8,128)(2,1)S(1)}, bf16[2,256,2048]{2,1,0:T(8,128)(2,1)}, u32[]{:S(2)}) copy-start(bf16[2,256,2048]{2,1,0:T(8,128)(2,1)} %d1_in.1) | copy-start | bytes 6291460
  156.3 3.5 %collective-permute-start = (bf16[1,2048,256]{2,1,0:T(8,128)(2,1)S(1)}, bf16[1,2048,256]{2,1,0:T(8,128)(2,1)S(1)}, u32[]{:S(2)}, u32[]{:S(2)}) collective-permute-start(bf16[1,2048,256]{2,1,0:T(8,128)(2,1)S(1)} %constant_dynamic-slice_fusion.2), channel_id=1, source_target_pairs={{0,1},{1,0},{2,3},{3,2},{4,5},{5,4},{6,7},{7,6},{8,9},{9,8},{10,11... | collective-permute-start | bytes 3145736 | tf_op jit(solution)/shard_map/ppermute | solution.py:723
  157.6 3.7 %collective-permute-start.1 = (bf16[1,2048,256]{2,1,0:T(8,128)(2,1)S(1)}, bf16[1,2048,256]{2,1,0:T(8,128)(2,1)S(1)}, u32[]{:S(2)}, u32[]{:S(2)}) collective-permute-start(bf16[1,2048,256]{2,1,0:T(8,128)(2,1)S(1)} %constant_dynamic-slice_fusion.1), channel_id=1, source_target_pairs={{0,1},{1,0},{2,3},{3,2},{4,5},{5,4},{6,7},{7,6},{8,9},{9,8},{10,11... | collective-permute-start | bytes 3145736 | tf_op jit(solution)/shard_map/ppermute | solution.py:723
  158.2 4.8 %collective-permute-start.2 = (bf16[1,256,2048]{2,1,0:T(8,128)(2,1)S(1)}, bf16[1,256,2048]{2,1,0:T(8,128)(2,1)}, u32[]{:S(2)}, u32[]{:S(2)}) collective-permute-start(bf16[1,256,2048]{2,1,0:T(8,128)(2,1)S(1)} %constant_dynamic-slice_fusion), channel_id=1, source_target_pairs={{0,1},{1,0},{2,3},{3,2},{4,5},{5,4},{6,7},{7,6},{8,9},{9,8},{10,11... | collective-permute-start | bytes 3145736 | tf_op jit(solution)/shard_map/ppermute | solution.py:723
  159.8 36.2 %copy-start.4 = (bf16[1,2048,256]{2,1,0:T(8,128)(2,1)}, bf16[1,2048,256]{2,1,0:T(8,128)(2,1)S(1)}, u32[]{:S(2)}) copy-start(bf16[1,2048,256]{2,1,0:T(8,128)(2,1)S(1)} %collective-permute-done.g2_in) | copy-start | bytes 3145732
  161.3 1.0 copy-start.5
  209.5 5.8 %copy-start.1 = (bf16[128,2048]{1,0:T(8,128)(2,1)S(1)}, bf16[128,2048]{1,0:T(8,128)(2,1)}, u32[]{:S(2)}) copy-start(bf16[128,2048]{1,0:T(8,128)(2,1)} %get-tuple-element.11) | copy-start | bytes 1572868
  209.5 47.1 %all-to-all-start.1 = ((bf16[128,24,512]{2,1,0:T(8,128)(2,1)}), bf16[128,24,512]{2,1,0:T(8,128)(2,1)}, u32[]{:S(2)}, u32[]{:S(2)}) async-start(bf16[128,24,512]{2,1,0:T(8,128)(2,1)} %bitcast.18), calls=%async_computation.1 | async-start | bytes 6291456 | tf_op jit(solution)/shard_map/all_to_all | solution.py:691
